TPU v7x, 32 devices: a whole 2x2x4 slice. The times are simulated.
32 devices in a mesh: rep: 2 (over x), fs: 4 (over z), tp: 4 (over y, core).
Axes of the slice: x: 2, y: 2, z: 4, core: 2. Of those that a mesh axis runs over, the one named last changes fastest.
Arguments:
- residual: bfloat16 [8, 768, 4, 512], P(('rep', 'fs'), None, None, 'tp'), may hold values from -6 to 6
- mixer_gain: float32 [4, 512], P(None, 'tp'), may hold values from 0.1 to 1.9
- pool_weight: float32 [4, 512, 512], P(None, 'fs', 'tp'), may hold values from -0.25 to 0.25
- pool_scale: float32 [4, 512], P(None, 'tp'), may hold values from 0.5 to 2
- channel_gain: float32 [4, 512], P(None, 'tp'), may hold values from 0.1 to 1.9
- gate_weight: float32 [2048, 6144], P('fs', 'tp'), may hold values from -0.125 to 0.125
- up_weight: float32 [2048, 6144], P('fs', 'tp'), may hold values from -0.125 to 0.125
- gate_scale: float32 [4, 1536], P('fs', 'tp'), may hold values from 0.5 to 2
- up_scale: float32 [4, 1536], P('fs', 'tp'), may hold values from 0.5 to 2
- gate_taps: float32 [3, 6144], P(None, 'tp'), may hold values from -3.5 to 3.5
- up_taps: float32 [3, 6144], P(None, 'tp'), may hold values from -3.5 to 3.5
- down_weight: float32 [6144, 2048], P('tp', 'fs'), may hold values from -0.078125 to 0.078125
- down_scale: float32 [4, 512], P(None, 'tp'), may hold values from 0.5 to 2
Outputs:
- layer_out: bfloat16 [8, 768, 4, 512], P(('rep', 'fs'), None, None, 'tp')
All inputs are finite; a program needn't handle non-finite values.
Results may differ from a plain program's by a relative error of at most 0.018.
Values may be sent and summed in bfloat16 or wider, within the bound.
A program may use at most 128 MiB of HBM per device.

v0:
```python
import functools

import jax
import jax.numpy as jnp
from jax import lax
from jax.experimental import pallas as pl
from jax.experimental.pallas import tpu as pltpu
from jax.sharding import PartitionSpec as P

WINDOWS = (2, 4, 8, 16)
EPSILON = 1e-05
SUBS = 2
COLUMNS = 256
F32 = jnp.float32
BF16 = jnp.bfloat16


def delayed(values, steps):
    rows = lax.broadcasted_iota(jnp.int32, values.shape, 0)
    return jnp.where(rows >= steps, pltpu.roll(values, steps, 0), 0.0)


def causal_taps(values, taps):
    return taps[2:3] * values + taps[1:2] * delayed(values, 1) + taps[0:1] * delayed(values, 2)


def block_kernel(
    sizes,
    residual,
    gains,
    pool_scale,
    down_scale,
    scale_pair,
    gate_taps,
    up_taps,
    pool_own,
    gate_own,
    up_own,
    down_own,
    out,
    pool_full,
    gate_full,
    up_full,
    down_full,
    gathered,
    middle_all,
    gains_all,
    scales_all,
    scale_row,
    pooled,
    middle,
    inputs,
    gate_pre,
    hidden,
    partials,
    arrived,
    ring_send,
    ring_recv,
    rep_send,
    rep_recv,
    pool_send,
    pool_recv,
    pool_rep_send,
    pool_rep_recv,
    scale_send,
    scale_recv,
    tp_send,
    tp_recv,
    part_send,
    part_recv,
    local_sem,
):
    n_rep, n_fs, n_tp = sizes
    rep, fs, tp = (lax.axis_index(name) for name in ("rep", "fs", "tp"))
    length = residual.shape[0]
    groups = pool_full.shape[0]
    channels = pool_full.shape[1]
    local = residual.shape[1] // groups
    width = groups * channels

    def other(axis, offset):
        me, count = {"rep": (rep, n_rep), "fs": (fs, n_fs), "tp": (tp, n_tp)}[axis]
        return lax.rem(me + offset, count)

    def remote(src, dst, send, recv, axis, offset):
        return pltpu.make_async_remote_copy(
            src_ref=src,
            dst_ref=dst,
            send_sem=send,
            recv_sem=recv,
            device_id={axis: other(axis, offset)},
            device_id_type=pl.DeviceIdType.MESH,
        )

    barrier = pltpu.get_barrier_semaphore()
    for axis, count in (("rep", n_rep), ("fs", n_fs), ("tp", n_tp)):
        for offset in range(1, count):
            pl.semaphore_signal(
                barrier,
                inc=1,
                device_id={axis: other(axis, offset)},
                device_id_type=pl.DeviceIdType.MESH,
            )
    pl.semaphore_wait(barrier, n_rep + n_fs + n_tp - 3)

    sent = []

    def start(copy, valid=None):
        sent.append((copy, valid))
        if valid is None:
            copy.start()
        else:
            pl.when(valid)(copy.start)

    weights = ((gate_own, gate_full), (up_own, up_full), (down_own, down_full))

    def piece(w, shard, half, sub, own=False):
        rows = weights[w][0].shape[0] // (n_rep * SUBS)
        part = pl.ds(pl.multiple_of((half * SUBS + sub) * rows, rows), rows)
        return weights[w][0].at[part] if own else weights[w][1].at[shard, part]

    def shard_sent(step, way):
        shard = fs + step if way else fs - step
        return jnp.clip(shard, 0, n_fs - 1), (shard <= n_fs - 1 if way else shard >= 0)

    def line(w, sub, step):
        for way in range(2):
            shard, valid = shard_sent(step, way)
            start(
                remote(
                    piece(w, shard, rep, sub, own=step == 0),
                    piece(w, shard, rep, sub),
                    ring_send.at[w, sub, 2 * step + way],
                    ring_recv.at[w, sub, 2 * step + way],
                    "fs",
                    n_fs - 1 if way else 1,
                ),
                valid & (fs > 0 if way else fs < n_fs - 1),
            )

    def serve(w, sub, step):
        for way in range(2):
            shard, valid = shard_sent(step + 1, way)
            mine = piece(w, shard, rep, sub)
            sems = (w, sub, 2 * step + way)
            pl.when(valid)(
                remote(
                    mine, mine, ring_send.at[sems], ring_recv.at[sems], "fs", 1
                ).wait_recv
            )
            if step < n_fs - 2:
                onward = (w, sub, 2 * step + 2 + way)
                start(
                    remote(
                        mine,
                        mine,
                        ring_send.at[onward],
                        ring_recv.at[onward],
                        "fs",
                        n_fs - 1 if way else 1,
                    ),
                    valid & (fs > 0 if way else fs < n_fs - 1),
                )
            for d in range(1, n_rep):
                start(
                    remote(
                        mine,
                        mine,
                        rep_send.at[sems + (d - 1,)],
                        rep_recv.at[sems + (d - 1,)],
                        "rep",
                        d,
                    ),
                    valid,
                )

    def settle(w, step, ways=(0, 1)):
        for way in ways:
            shard, valid = shard_sent(step + 1, way)

            @pl.when(valid)
            def _():
                for sub in range(SUBS):
                    for d in range(1, n_rep):
                        got = piece(w, shard, other("rep", n_rep - d), sub)
                        sems = (w, sub, 2 * step + way, d - 1)
                        remote(
                            got, got, rep_send.at[sems], rep_recv.at[sems], "rep", d
                        ).wait_recv()

    def local_copy(src, dst, idx):
        copy = pltpu.make_async_copy(src, dst, local_sem.at[idx])
        copy.start()
        return copy

    own_copies = [
        local_copy(residual, gathered.at[tp], 0),
        local_copy(gains, gains_all.at[tp], 1),
        local_copy(scale_pair, scales_all.at[fs], 2),
        local_copy(gate_own, gate_full.at[fs], 3),
        local_copy(up_own, up_full.at[fs], 4),
        local_copy(down_own, down_full.at[fs], 5),
    ]

    pool_rows = pool_own.shape[1]
    rep_groups = groups // n_rep

    def pool_part(shard, half):
        return pool_full.at[
            pl.ds(half * rep_groups, rep_groups),
            pl.ds(pl.multiple_of(shard * pool_rows, pool_rows), pool_rows),
        ]

    pool_copy = local_copy(
        pool_own, pool_full.at[:, pl.ds(pl.multiple_of(fs * pool_rows, pool_rows), pool_rows)], 6
    )

    for d in range(1, n_fs):
        start(
            remote(
                pool_own.at[pl.ds(rep * rep_groups, rep_groups)],
                pool_part(fs, rep),
                pool_send.at[d - 1],
                pool_recv.at[d - 1],
                "fs",
                d,
            )
        )
    for w in (0, 1):
        for sub in range(SUBS):
            if n_fs > 1:
                line(w, sub, 0)
    for d in range(1, n_tp):
        start(remote(gains, gains_all.at[tp], tp_send.at[0, d - 1], tp_recv.at[0, d - 1], "tp", d))
    for d in range(1, n_tp):
        start(
            remote(residual, gathered.at[tp], tp_send.at[1, d - 1], tp_recv.at[1, d - 1], "tp", d)
        )
    for d in range(1, n_fs):
        start(
            remote(
                scale_pair, scales_all.at[fs], scale_send.at[d - 1], scale_recv.at[d - 1], "fs", d
            )
        )

    for d in range(1, n_fs):
        shard = other("fs", n_fs - d)
        mine = pool_part(shard, rep)
        remote(mine, mine, pool_send.at[d - 1], pool_recv.at[d - 1], "fs", d).wait_recv()
        for e in range(1, n_rep):
            start(
                remote(
                    mine,
                    mine,
                    pool_rep_send.at[d - 1, e - 1],
                    pool_rep_recv.at[d - 1, e - 1],
                    "rep",
                    e,
                )
            )
    for d in range(1, n_fs):
        shard = other("fs", n_fs - d)
        for e in range(1, n_rep):
            got = pool_part(shard, other("rep", n_rep - e))
            remote(
                got,
                got,
                pool_rep_send.at[d - 1, e - 1],
                pool_rep_recv.at[d - 1, e - 1],
                "rep",
                e,
            ).wait_recv()
    pool_copy.wait()
    for copy in own_copies:
        copy.wait()

    def tp_arrivals(idx, buffer):
        for d in range(1, n_tp):
            got = buffer.at[other("tp", n_tp - d)]
            remote(got, got, tp_send.at[idx, d - 1], tp_recv.at[idx, d - 1], "tp", d).wait_recv()

    for sub in range(SUBS):
        serve(0, sub, 0)
    tp_arrivals(0, gains_all)
    tp_arrivals(1, gathered)
    for sub in range(SUBS):
        serve(1, sub, 0)

    def mean_square_root(buffer):
        total = jnp.zeros((length, 1), F32)
        for t in range(n_tp):
            values = buffer[t].astype(F32)
            total = total + jnp.sum(values * values, axis=1, keepdims=True)
        return lax.rsqrt(total / width + EPSILON)

    factor = mean_square_root(gathered)
    positions = lax.broadcasted_iota(jnp.int32, (length, 1), 0).astype(F32) + 1.0
    for g in range(groups):
        part = slice(g * local, (g + 1) * local)
        share = 1.0 / jnp.minimum(positions, float(WINDOWS[g]))
        for t in range(n_tp):
            values = gathered[t, :, part].astype(F32)
            normed = (values * factor * gains_all[t, 0:1, part]).astype(BF16).astype(F32)
            totals = normed
            reach = 1
            while reach < WINDOWS[g]:
                totals = totals + delayed(totals, reach)
                reach = reach * 2
            pooled[:, t * local : (t + 1) * local] = (totals * share - normed).astype(BF16)
        mixed = jnp.dot(pooled[...], pool_full[g], preferred_element_type=F32)
        middle[:, part] = (
            mixed * pool_scale[:, part] + residual[:, part].astype(F32)
        ).astype(BF16)

    middle_copy = local_copy(middle, middle_all.at[tp], 0)
    for d in range(1, n_tp):
        start(
            remote(middle, middle_all.at[tp], tp_send.at[2, d - 1], tp_recv.at[2, d - 1], "tp", d)
        )
    for step in range(1, n_fs - 1):
        for w in (0, 1):
            if step == n_fs - 2 and n_fs > 2:
                break
            for sub in range(SUBS):
                serve(w, sub, step)
    for sub in range(SUBS):
        if n_fs > 1:
            line(2, sub, 0)
    for d in range(1, n_fs):
        got = scales_all.at[other("fs", n_fs - d)]
        remote(got, got, scale_send.at[d - 1], scale_recv.at[d - 1], "fs", d).wait_recv()
    shard_columns = scale_pair.shape[1]
    for f in range(n_fs):
        scale_row[:, f * shard_columns : (f + 1) * shard_columns] = scales_all[f]

    middle_copy.wait()
    tp_arrivals(2, middle_all)
    factor = mean_square_root(middle_all)
    for t in range(n_tp):
        for g in range(groups):
            part = slice(g * local, (g + 1) * local)
            start_column = g * channels + t * local
            inputs[:, start_column : start_column + local] = (
                middle_all[t, :, part].astype(F32) * factor * gains_all[t, 1:2, part]
            ).astype(BF16)

    def finish(w):
        if n_fs > 2:
            for sub in range(SUBS):
                serve(w, sub, n_fs - 2)
        for step in range(n_fs - 1):
            settle(w, step)

    def product(full, columns, row):
        block = full[:, :, columns].reshape(width, COLUMNS)
        made = jnp.dot(inputs[...], block, preferred_element_type=F32)
        return (made * scale_row[row : row + 1, columns]).astype(BF16)

    chunks = gate_full.shape[2] // COLUMNS

    finish(0)

    @pl.loop(0, chunks)
    def _(j):
        columns = pl.ds(pl.multiple_of(j * COLUMNS, COLUMNS), COLUMNS)
        gate_pre[:, columns] = product(gate_full, columns, 0)

    finish(1)
    for sub in range(SUBS):
        if n_fs > 1:
            serve(2, sub, 0)

    @pl.loop(0, chunks)
    def _(j):
        columns = pl.ds(pl.multiple_of(j * COLUMNS, COLUMNS), COLUMNS)
        up_values = product(up_full, columns, 1).astype(F32)
        conv_gate = causal_taps(gate_pre[:, columns].astype(F32), gate_taps[:, columns])
        conv_up = causal_taps(up_values, up_taps[:, columns])
        silu = conv_gate / (1.0 + jnp.exp(-conv_gate))
        hidden[:, columns] = (silu * conv_up).astype(BF16)

    shard_width = down_own.shape[1]

    def to_peers(idx, src, dst):
        for d in range(1, n_tp):
            start(
                remote(
                    src(other("tp", d)),
                    dst(tp),
                    part_send.at[idx, d - 1],
                    part_recv.at[idx, d - 1],
                    "tp",
                    d,
                )
            )

    def from_peers(idx, dst):
        for d in range(1, n_tp):
            got = dst(other("tp", n_tp - d))
            remote(
                got, got, part_send.at[idx, d - 1], part_recv.at[idx, d - 1], "tp", d
            ).wait_recv()

    def conclude(g, columns):
        total = partials[tp, g].astype(F32)
        for d in range(1, n_tp):
            total = total + arrived[other("tp", d), g].astype(F32)
        out[:, columns] = (
            total * down_scale[:, columns] + middle[:, columns].astype(F32)
        ).astype(BF16)

    if shard_width == channels and local % 128 == 0:
        def share(shard):
            made = jnp.dot(hidden[...], down_full[shard], preferred_element_type=F32)
            for t in range(n_tp):
                partials[t, shard] = made[:, t * local : (t + 1) * local].astype(BF16)
            for d in range(1, n_tp):
                peer = other("tp", d)
                remote(
                    partials.at[peer, shard],
                    arrived.at[tp, shard],
                    part_send.at[shard, d - 1],
                    part_recv.at[shard, d - 1],
                    "tp",
                    d,
                ).start()

        share(fs)
        for step in range(n_fs - 1):
            if step >= 1:
                for sub in range(SUBS):
                    serve(2, sub, step)
            for way in range(2):
                settle(2, step, (way,))
                shard, valid = shard_sent(step + 1, way)
                pl.when(valid)(functools.partial(share, shard))
        for shard in range(n_fs):
            from_peers(shard, lambda t: arrived.at[t, shard])
            conclude(shard, slice(shard * local, (shard + 1) * local))
            for d in range(1, n_tp):
                mine = partials.at[other("tp", d), shard]
                remote(
                    mine, mine, part_send.at[shard, d - 1], part_recv.at[shard, d - 1], "tp", d
                ).wait_send()
    else:
        for step in range(n_fs - 1):
            if step >= 1:
                for sub in range(SUBS):
                    serve(2, sub, step)
            settle(2, step)
        for f in range(n_fs):
            made = jnp.dot(hidden[...], down_full[f], preferred_element_type=F32).astype(BF16)
            span = min(local, shard_width)
            for at in range(0, shard_width, span):
                g, channel = divmod(f * shard_width + at, channels)
                t, low = divmod(channel, local)
                partials[t, g, :, low : low + span] = made[:, at : at + span]
        to_peers(0, lambda t: partials.at[t], lambda t: arrived.at[t])
        from_peers(0, lambda t: arrived.at[t])
        for g in range(groups):
            conclude(g, slice(g * local, (g + 1) * local))

    for copy, valid in sent:
        if valid is None:
            copy.wait_send()
        else:
            pl.when(valid)(copy.wait_send)


def shards(
    sizes,
    residual,
    mixer_gain,
    pool_weight,
    pool_scale,
    channel_gain,
    gate_weight,
    up_weight,
    gate_scale,
    up_scale,
    gate_taps,
    up_taps,
    down_weight,
    down_scale,
):
    n_rep, n_fs, n_tp = sizes
    _, length, groups, local = residual.shape
    channels = local * n_tp
    width = groups * channels
    own_width = groups * local
    hidden_width = gate_weight.shape[1]
    vmem = pl.BlockSpec(memory_space=pltpu.VMEM)
    anywhere = pl.BlockSpec(memory_space=pl.ANY)
    dma = pltpu.SemaphoreType.DMA
    hops = max(n_fs - 1, 1)
    reps = max(n_rep - 1, 1)
    peers = max(n_tp - 1, 1)
    out = pl.pallas_call(
        functools.partial(block_kernel, sizes),
        out_shape=jax.ShapeDtypeStruct((length, own_width), BF16),
        in_specs=[vmem] * 8 + [anywhere] * 3,
        out_specs=vmem,
        scratch_shapes=[
            pltpu.VMEM((groups, channels, local), BF16),
            pltpu.VMEM((n_fs,) + gate_weight.shape, BF16),
            pltpu.VMEM((n_fs,) + up_weight.shape, BF16),
            pltpu.VMEM((n_fs,) + down_weight.shape, BF16),
            pltpu.VMEM((n_tp, length, own_width), BF16),
            pltpu.VMEM((n_tp, length, own_width), BF16),
            pltpu.VMEM((n_tp, 2, own_width), F32),
            pltpu.VMEM((n_fs, 2, gate_scale.shape[1]), F32),
            pltpu.VMEM((2, hidden_width), F32),
            pltpu.VMEM((length, channels), BF16),
            pltpu.VMEM((length, own_width), BF16),
            pltpu.VMEM((length, width), BF16),
            pltpu.VMEM((length, hidden_width), BF16),
            pltpu.VMEM((length, hidden_width), BF16),
            pltpu.VMEM((n_tp, groups, length, local), BF16),
            pltpu.VMEM((n_tp, groups, length, local), BF16),
            dma((3, SUBS, 2 * hops)),
            dma((3, SUBS, 2 * hops)),
            dma((3, SUBS, 2 * hops, reps)),
            dma((3, SUBS, 2 * hops, reps)),
            dma((hops,)),
            dma((hops,)),
            dma((hops, reps)),
            dma((hops, reps)),
            dma((hops,)),
            dma((hops,)),
            dma((3, peers)),
            dma((3, peers)),
            dma((n_fs, peers)),
            dma((n_fs, peers)),
            dma((7,)),
        ],
        compiler_params=pltpu.CompilerParams(
            collective_id=0, has_side_effects=True, vmem_limit_bytes=60 * 1024 * 1024
        ),
    )(
        residual.reshape(length, own_width),
        jnp.stack([mixer_gain.reshape(-1), channel_gain.reshape(-1)]),
        pool_scale.reshape(1, -1),
        down_scale.reshape(1, -1),
        jnp.concatenate([gate_scale, up_scale], axis=0),
        gate_taps,
        up_taps,
        pool_weight.astype(BF16),
        gate_weight.astype(BF16),
        up_weight.astype(BF16),
        down_weight.astype(BF16),
    )
    return out.reshape(1, length, groups, local)


def solution(mesh):
    placed = (
        P(("rep", "fs"), None, None, "tp"),
        P(None, "tp"),
        P(None, "fs", "tp"),
        P(None, "tp"),
        P(None, "tp"),
        P("fs", "tp"),
        P("fs", "tp"),
        P("fs", "tp"),
        P("fs", "tp"),
        P(None, "tp"),
        P(None, "tp"),
        P("tp", "fs"),
        P(None, "tp"),
    )
    sizes = tuple(mesh.shape[name] for name in ("rep", "fs", "tp"))
    return jax.shard_map(
        functools.partial(shards, sizes),
        mesh=mesh,
        in_specs=placed,
        out_specs=P(("rep", "fs"), None, None, "tp"),
        check_vma=False,
    )
```

profile of v0, /device:TPU:0, one launch (start us, length us, event | category | flops | bytes accessed | tf_op | source)
XLA Modules:
  0.0 214.5 jit_solution(10177358644888191833)
XLA Ops:
  0.0 1.3 pad_maximum_fusion.1.scale_pair
  1.3 1.3 pad_maximum_fusion.gains
  2.6 1.6 convert_element_type.12.pool_own
  4.2 0.0 copy-start
  4.2 2.3 %copy.16 = bf16[96,8,4,128]{3,1,2,0:T(8,128)(2,1)} copy(bf16[96,8,4,128]{3,2,1,0:T(4,128)(2,1)} %bitcast.10) | data formatting | bytes 1572864
  6.5 3.2 %convert_element_type.13.gate_own = bf16[512,1536]{1,0:T(8,128)(2,1)} convert(f32[512,1536]{1,0:T(8,128)} %param.18) | non-fusion elementwise | flops 786432 | bytes 4718592 | tf_op jit(solution)/shard_map/convert_element_type | solution.py:548
  9.7 0.0 copy-done
  9.7 0.0 copy-start.1
  9.7 1.3 convert_element_type.14.up_own
  11.1 1.1 copy-done.1
  12.2 1.3 convert_element_type.15.down_own
  13.5 198.5 %shard_map.127 = bf16[768,512]{1,0:T(8,128)(2,1)} custom-call(bf16[768,512]{1,0:T(8,128)(2,1)} %bitcast.9, f32[2,512]{1,0:T(2,128)} %pad_maximum_fusion.gains, f32[1,512]{1,0:T(1,128)} %bitcast.11, f32[1,512]{1,0:T(1,128)} %bitcast.12, f32[2,384]{1,0:T(2,128)} %pad_maximum_fusion.1.scale_pair, f32[3,1536]{1,0:T(4,128)} %gate_taps.1, f32[3,1536]{1,0:T(4,128)} %up_taps.1, ...), custom_call_target="tpu_custom_call" | custom-call | tf_op jit(solution)/shard_map/pallas_call | solution.py:498
  212.1 2.4 %reshape.15 = bf16[1,768,4,128]{3,2,1,0:T(4,128)(2,1)} reshape(bf16[768,512]{1,0:T(8,128)(2,1)} %shard_map.127) | data formatting | bytes 1572864 | tf_op jit(solution)/shard_map/reshape | solution.py:552
Async XLA Ops:
  4.2 5.5 %copy-start = (f32[512,1536]{1,0:T(8,128)S(1)}, f32[512,1536]{1,0:T(8,128)}, u32[]{:S(2)}) copy-start(f32[512,1536]{1,0:T(8,128)} %param.19) | copy-start | bytes 9437188
  9.7 2.5 %copy-start.1 = (f32[1536,512]{1,0:T(8,128)S(1)}, f32[1536,512]{1,0:T(8,128)}, u32[]{:S(2)}) copy-start(f32[1536,512]{1,0:T(8,128)} %param.24) | copy-start | bytes 9437188
where the time goes:
time: 216 us; the launch traced here: 215 us
  Pallas kernels  199 us (92%)
  other arithmetic  10.1 us (5%)
  local copies, waits for them, and re-layouts  5.87 us (3%)
    pallas_call x1, Pallas kernels, shards(): pl.pallas_call(functools.partial(block_kernel, sizes), out_shape=jax.Shap...  199 us

commit v1 on v0

--- a/solution.py
+++ b/solution.py
@@ -11,6 +11,7 @@
 EPSILON = 1e-05
 SUBS = 2
 COLUMNS = 256
+VMEM_BYTES = 62 * 1024 * 1024
 F32 = jnp.float32
 BF16 = jnp.bfloat16
 
@@ -467,6 +468,633 @@
             pl.when(valid)(copy.wait_send)
 
 
+BAND = 256
+PIECES = 4
+TOKEN_PARTS = 2
+
+
+def pair_kernel(
+    residual,
+    mixer_gain,
+    pool_scale,
+    channel_gain,
+    down_scale,
+    gate_scale,
+    up_scale,
+    gate_taps,
+    up_taps,
+    pool_own,
+    gate_own,
+    up_own,
+    down_own,
+    out,
+    stage_own,
+    stage_other,
+    stage_down,
+    stage_down_other,
+    stage_pool,
+    tokens,
+    small_all,
+    scales_all,
+    pool_near,
+    pool_full,
+    weights,
+    other,
+    down_full,
+    down_other,
+    normed,
+    pooled,
+    inputs,
+    middle,
+    hidden,
+    keep,
+    give,
+    got,
+    y_out,
+    y_in,
+    z_out,
+    z_in,
+    small_send,
+    small_recv,
+    scale_send,
+    scale_recv,
+    pz_send,
+    pz_recv,
+    px_send,
+    px_recv,
+    pt_send,
+    pt_recv,
+    rz_send,
+    rz_recv,
+    ry_send,
+    ry_recv,
+    rs_send,
+    rs_recv,
+    gz_send,
+    gz_recv,
+    gx_send,
+    gx_recv,
+    dz_send,
+    dz_recv,
+    dx_send,
+    dx_recv,
+    core_send,
+    core_recv,
+    y_send,
+    y_recv,
+    z_send,
+    z_recv,
+    local_sem,
+):
+    rep, fs, tp = (lax.axis_index(name) for name in ("rep", "fs", "tp"))
+    length = residual.shape[0]
+    groups, pool_rows, local = pool_own.shape
+    channels = pool_full.shape[1]
+    width = groups * channels
+    rows = gate_own.shape[0]
+    half_rows = rows // 2
+    half_hidden = gate_own.shape[1] // 2
+    chunks = half_hidden // 128
+    half_columns = down_own.shape[1] // 2
+    member = lax.rem(fs, 2)
+    side = tp // 2
+    core = lax.rem(tp, 2)
+    sibling = {"tp": tp + 1 - 2 * core}
+    across = {"tp": lax.rem(tp + 2, 4)}
+    diagonal = {"tp": 3 - tp}
+    mirror = {"rep": 1 - rep}
+    same, far, partner = lax.rem(fs + 2, 4), 3 - fs, fs + 1 - 2 * member
+    sources = (same, far, partner)
+    outer = (fs == 0) | (fs == 3)
+
+    sent = []
+
+    def remote(src, dst, send, recv, device):
+        return pltpu.make_async_remote_copy(
+            src_ref=src,
+            dst_ref=dst,
+            send_sem=send,
+            recv_sem=recv,
+            device_id=device,
+            device_id_type=pl.DeviceIdType.MESH,
+        )
+
+    def start(*parts):
+        copy = remote(*parts)
+        sent.append(copy)
+        copy.start()
+
+    def aligned(at, size):
+        return pl.ds(pl.multiple_of(at, size), size)
+
+    def local_copy(src, dst, idx):
+        copy = pltpu.make_async_copy(src, dst, local_sem.at[idx])
+        copy.start()
+        return copy
+
+    mine = aligned(member * half_hidden, half_hidden)
+    theirs = aligned((1 - member) * half_hidden, half_hidden)
+    rep_rows = aligned(rep * half_rows, half_rows)
+    rep_columns = aligned(rep * half_columns, half_columns)
+    load_tokens = local_copy(residual, tokens.at[0, tp], 0)
+    load_pool = local_copy(pool_own, stage_pool, 1)
+    loads = [
+        local_copy(gate_own.at[:, mine], stage_own.at[0], 2),
+        local_copy(up_own.at[:, mine], stage_own.at[1], 3),
+        local_copy(gate_own.at[rep_rows, theirs], stage_other.at[0], 4),
+        local_copy(up_own.at[rep_rows, theirs], stage_other.at[1], 5),
+    ]
+    load_down = [
+        local_copy(down_own.at[mine], stage_down, 6),
+        local_copy(down_own.at[theirs, rep_columns], stage_down_other, 7),
+    ]
+
+    barrier = pltpu.get_barrier_semaphore()
+    peers = (mirror, sibling, across, diagonal) + tuple({"fs": f} for f in sources)
+    for device in peers:
+        pl.semaphore_signal(
+            barrier, inc=1, device_id=device, device_id_type=pl.DeviceIdType.MESH
+        )
+    small_all[tp, 0] = mixer_gain[...]
+    small_all[tp, 1] = pool_scale[...]
+    small_all[tp, 2] = channel_gain[...]
+    scales_all[fs, 0] = gate_scale[...]
+    scales_all[fs, 1] = up_scale[...]
+    load_pool.wait()
+    pool_near[...] = stage_pool[...].astype(BF16)
+    load_tokens.wait()
+    pl.semaphore_wait(barrier, len(peers))
+
+    def token_part(slot, t, part):
+        span = length // TOKEN_PARTS
+        return tokens.at[slot, t, pl.ds(part * span, span)]
+
+    def pool_part(shard, half):
+        span = groups // 2
+        return pool_full.at[
+            pl.ds(half * span, span),
+            aligned(shard * pool_rows, pool_rows),
+            aligned(tp * local, local),
+        ]
+
+    for q, f in enumerate(sources):
+        start(
+            pool_near.at[pl.ds(rep * (groups // 2), groups // 2)],
+            pool_part(fs, rep),
+            pz_send.at[q],
+            pz_recv.at[q],
+            {"fs": f},
+        )
+    for part in range(TOKEN_PARTS):
+        piece = token_part(0, tp, part)
+        start(piece, piece, ry_send.at[0, part], ry_recv.at[0, part], across)
+        start(piece, piece, rs_send.at[0, part], rs_recv.at[0, part], sibling)
+    for at, values in enumerate((mixer_gain, pool_scale, channel_gain)):
+        for q, device in enumerate((sibling, across, diagonal)):
+            start(values, small_all.at[tp, at], small_send.at[at, q], small_recv.at[at, q], device)
+    for at, values in enumerate((gate_scale, up_scale)):
+        for q, f in enumerate(sources):
+            start(
+                values, scales_all.at[fs, at], scale_send.at[at, q], scale_recv.at[at, q], {"fs": f}
+            )
+    pool_copy = local_copy(
+        pool_near,
+        pool_full.at[:, aligned(fs * pool_rows, pool_rows), aligned(tp * local, local)],
+        8,
+    )
+
+    def chunk_target(j, shard, half):
+        return weights.at[j, shard, aligned(half * half_rows, half_rows)]
+
+    def chunk_copies(j):
+        target = chunk_target(j, fs, rep)
+        return [
+            remote(source, target, gz_send.at[j, q], gz_recv.at[j, q], {"fs": f})
+            for q, (source, f) in enumerate(
+                ((target, same), (other.at[j], far), (other.at[j], partner))
+            )
+        ]
+
+    for load in loads:
+        load.wait()
+
+    @pl.loop(0, chunks)
+    def _(j):
+        columns = aligned(j * 128, 128)
+        for at in range(2):
+            lanes = slice(at * 128, (at + 1) * 128)
+            weights[j, fs, :, lanes] = stage_own[at, :, columns].astype(BF16)
+            other[j, :, lanes] = stage_other[at, :, columns].astype(BF16)
+        for copy in chunk_copies(j):
+            copy.start()
+
+        @pl.when(j == 0)
+        def _():
+            for part in range(TOKEN_PARTS):
+                remote(
+                    token_part(0, tp, part),
+                    token_part(1, tp, part),
+                    rz_send.at[part],
+                    rz_recv.at[part],
+                    {"fs": partner},
+                ).start()
+
+    for load in load_down:
+        load.wait()
+    for half in range(2):
+        down_full[fs, half] = stage_down[
+            :, half * half_columns : (half + 1) * half_columns
+        ].astype(BF16)
+    down_other[...] = stage_down_other[...].astype(BF16)
+
+    def down_part(shard, half, sub):
+        span = half_hidden // PIECES
+        return down_full.at[shard, half, pl.ds(sub * span, span)]
+
+    for q, f in enumerate(sources):
+        for sub in range(PIECES):
+            span = half_hidden // PIECES
+            source = (
+                down_part(fs, rep, sub) if q == 0 else down_other.at[pl.ds(sub * span, span)]
+            )
+            start(
+                source,
+                down_part(fs, rep, sub),
+                dz_send.at[q, sub],
+                dz_recv.at[q, sub],
+                {"fs": f},
+            )
+
+    def landed(ref, send, recv):
+        remote(ref, ref, send, recv, mirror).wait_recv()
+
+    for q, f in enumerate(sources):
+        piece = pool_part(f, rep)
+        landed(piece, pz_send.at[q], pz_recv.at[q])
+        start(piece, piece, px_send.at[q], px_recv.at[q], mirror)
+    for q, f in enumerate(sources):
+        landed(pool_part(f, 1 - rep), px_send.at[q], px_recv.at[q])
+    pool_copy.wait()
+
+    def pool_slab(t):
+        return pool_full.at[:, :, aligned(t * local, local)]
+
+    slab = pool_slab(tp)
+    start(slab, slab, pt_send.at[1], pt_recv.at[1], across)
+    start(slab, slab, pt_send.at[0], pt_recv.at[0], sibling)
+
+    def forward_chunk(j, do_start):
+        for q, f in enumerate(sources):
+            piece = chunk_target(j, f, rep)
+            landed(piece, gz_send.at[j, q], gz_recv.at[j, q])
+            do_start(piece, piece, gx_send.at[j, q], gx_recv.at[j, q], mirror)
+
+    t_sibling, t_across, t_diagonal = sibling["tp"], across["tp"], diagonal["tp"]
+    for part in range(TOKEN_PARTS):
+        piece = token_part(0, t_across, part)
+        landed(piece, ry_send.at[0, part], ry_recv.at[0, part])
+        start(piece, piece, rs_send.at[1, part], rs_recv.at[1, part], sibling)
+    forward_chunk(0, start)
+    for part in range(TOKEN_PARTS):
+        piece = token_part(1, tp, part)
+        landed(piece, rz_send.at[part], rz_recv.at[part])
+        start(piece, piece, ry_send.at[1, part], ry_recv.at[1, part], across)
+        start(piece, piece, rs_send.at[2, part], rs_recv.at[2, part], sibling)
+    slab = pool_slab(t_across)
+    landed(slab, pt_send.at[1], pt_recv.at[1])
+    start(slab, slab, pt_send.at[2], pt_recv.at[2], sibling)
+    for part in range(TOKEN_PARTS):
+        landed(token_part(0, t_sibling, part), rs_send.at[0, part], rs_recv.at[0, part])
+        landed(token_part(0, t_diagonal, part), rs_send.at[1, part], rs_recv.at[1, part])
+    for at in range(3):
+        for q, t in enumerate((t_sibling, t_across, t_diagonal)):
+            landed(small_all.at[t, at], small_send.at[at, q], small_recv.at[at, q])
+    landed(pool_slab(t_sibling), pt_send.at[0], pt_recv.at[0])
+    landed(pool_slab(t_diagonal), pt_send.at[2], pt_recv.at[2])
+
+    positions = lax.broadcasted_iota(jnp.int32, (BAND, 1), 0).astype(F32) + 1.0
+    distance = (
+        lax.broadcasted_iota(jnp.int32, (BAND, 2 * BAND), 0)
+        + BAND
+        - lax.broadcasted_iota(jnp.int32, (BAND, 2 * BAND), 1)
+    )
+
+    def mix(slot):
+        span = slice(slot * length, (slot + 1) * length)
+        square = jnp.zeros((length, local), F32)
+        for t in range(4):
+            for g in range(groups):
+                values = tokens[slot, t, :, g * local : (g + 1) * local].astype(F32)
+                square = square + values * values
+        factor = lax.rsqrt(jnp.sum(square, axis=1, keepdims=True) / width + EPSILON)
+        square = jnp.zeros((length, local), F32)
+        for g in range(groups):
+            part = slice(g * local, (g + 1) * local)
+            for t in range(4):
+                values = tokens[slot, t, :, part].astype(F32)
+                normed[:, t * local : (t + 1) * local] = (
+                    values * factor * small_all[t, 0, g : g + 1]
+                ).astype(BF16)
+            band = jnp.where((distance >= 0) & (distance < WINDOWS[g]), 1.0, 0.0).astype(BF16)
+            for b in range(length // BAND):
+                here = slice(b * BAND, (b + 1) * BAND)
+                if b == 0:
+                    totals = jnp.dot(band[:, BAND:], normed[here], preferred_element_type=F32)
+                    totals = totals / jnp.minimum(positions, float(WINDOWS[g]))
+                else:
+                    totals = jnp.dot(
+                        band,
+                        normed[(b - 1) * BAND : (b + 1) * BAND],
+                        preferred_element_type=F32,
+                    ) * (1.0 / WINDOWS[g])
+                pooled[here] = (totals - normed[here].astype(F32)).astype(BF16)
+            mixed = jnp.dot(pooled[...], pool_full[g], preferred_element_type=F32)
+            for t in range(4):
+                made = (
+                    mixed[:, t * local : (t + 1) * local] * small_all[t, 1, g : g + 1]
+                    + tokens[slot, t, :, part].astype(F32)
+                ).astype(BF16)
+                inputs[span, g * channels + t * local : g * channels + (t + 1) * local] = made
+                values = made.astype(F32)
+                square = square + values * values
+        factor = lax.rsqrt(jnp.sum(square, axis=1, keepdims=True) / width + EPSILON)
+        if slot == 0:
+            for g in range(groups):
+                middle[:, g * local : (g + 1) * local] = inputs[
+                    span, aligned(g * channels + tp * local, local)
+                ]
+        for g in range(groups):
+            for t in range(4):
+                columns = slice(g * channels + t * local, g * channels + (t + 1) * local)
+                inputs[span, columns] = (
+                    inputs[span, columns].astype(F32) * factor * small_all[t, 2, g : g + 1]
+                ).astype(BF16)
+
+    mix(0)
+    forward_chunk(1, start)
+    for part in range(TOKEN_PARTS):
+        piece = token_part(1, t_across, part)
+        landed(piece, ry_send.at[1, part], ry_recv.at[1, part])
+        start(piece, piece, rs_send.at[3, part], rs_recv.at[3, part], sibling)
+    for part in range(TOKEN_PARTS):
+        landed(token_part(1, t_sibling, part), rs_send.at[2, part], rs_recv.at[2, part])
+        landed(token_part(1, t_diagonal, part), rs_send.at[3, part], rs_recv.at[3, part])
+    forward_chunk(2, start)
+    mix(1)
+    forward_chunk(3, start)
+    for at in range(2):
+        for q, f in enumerate(sources):
+            landed(scales_all.at[f, at], scale_send.at[at, q], scale_recv.at[at, q])
+
+    ahead = 4
+    thirds = scales_all.shape[3] // 128
+
+    def start_only(*parts):
+        remote(*parts).start()
+
+    @pl.loop(0, chunks)
+    def _(j):
+        for q, f in enumerate(sources):
+            landed(chunk_target(j, f, 1 - rep), gx_send.at[j, q], gx_recv.at[j, q])
+        here = aligned(member * half_hidden + j * 128, 128)
+        unit = member * chunks + j
+        scale_at = aligned(lax.rem(unit, thirds) * 128, 128)
+        taps = [
+            table[:, here] * scales_all[unit // thirds, at, :, scale_at]
+            for at, table in enumerate((gate_taps, up_taps))
+        ]
+        block = weights[j].reshape(width, 256)
+        for slot in range(2):
+            span = slice(slot * length, (slot + 1) * length)
+            made = jnp.dot(inputs[span], block, preferred_element_type=F32)
+            conv_gate = causal_taps(made[:, :128], taps[0])
+            conv_up = causal_taps(made[:, 128:], taps[1])
+            silu = conv_gate / (1.0 + jnp.exp(-conv_gate))
+            hidden[span, aligned(j * 128, 128)] = (silu * conv_up).astype(BF16)
+
+        @pl.when(j + ahead < chunks)
+        def _():
+            forward_chunk(j + ahead, start_only)
+
+    kinds = (jnp.where(outer, 2, 1), jnp.int32(0), jnp.where(outer, 1, 2))
+    shard_order = (
+        fs,
+        jnp.where(outer, partner, far),
+        same,
+        jnp.where(outer, far, partner),
+    )
+
+    def product(shard, half):
+        for slot in (1, 0):
+            span = slice(slot * length, (slot + 1) * length)
+            made = jnp.dot(hidden[span], down_full[shard, half], preferred_element_type=F32)
+            low, high = made[:, :local], made[:, local:]
+            keep[shard, half, span] = jnp.where(core == 0, low, high)
+            give[shard, half, span] = jnp.where(core == 0, high, low).astype(BF16)
+        start(
+            give.at[shard, half],
+            got.at[shard, half],
+            core_send.at[shard, half],
+            core_recv.at[shard, half],
+            sibling,
+        )
+
+    def y_copy(shard):
+        return remote(y_out.at[shard], y_in.at[shard], y_send.at[shard], y_recv.at[shard], across)
+
+    def join_cores(shard, half):
+        landed(got.at[shard, half], core_send.at[shard, half], core_recv.at[shard, half])
+        total = keep[shard, half] + got[shard, half].astype(F32)
+
+        @pl.when(half == side)
+        def _():
+            keep[shard, half] = total
+
+        @pl.when(half != side)
+        def _():
+            y_out[shard] = total.astype(BF16)
+            y_copy(shard).start()
+
+    def join_sides(shard):
+        landed(y_in.at[shard], y_send.at[shard], y_recv.at[shard])
+        total = keep[shard, side] + y_in[shard].astype(F32)
+        z_out[shard] = total[length:].astype(BF16)
+        start(
+            z_out.at[shard],
+            z_in.at[shard],
+            z_send.at[shard],
+            z_recv.at[shard],
+            {"fs": partner},
+        )
+        keep[shard, side, :length] = total[:length]
+
+    def conclude(shard):
+        landed(z_in.at[shard], z_send.at[shard], z_recv.at[shard])
+        columns = aligned(shard * local, local)
+        total = keep[shard, side, :length] + z_in[shard].astype(F32)
+        out[:, columns] = (
+            total * down_scale[pl.ds(shard, 1), :] + middle[:, columns].astype(F32)
+        ).astype(BF16)
+
+    product(fs, rep)
+    product(fs, 1 - rep)
+    join_cores(fs, rep)
+    for k in range(1, 4):
+        shard, q = shard_order[k], kinds[k - 1]
+        before = shard_order[k - 1]
+        for sub in range(PIECES):
+            piece = down_part(shard, rep, sub)
+            landed(piece, dz_send.at[q, sub], dz_recv.at[q, sub])
+            start(piece, piece, dx_send.at[q, sub], dx_recv.at[q, sub], mirror)
+        product(shard, rep)
+        join_cores(before, 1 - rep)
+        for sub in range(PIECES):
+            landed(
+                down_part(shard, 1 - rep, sub), dx_send.at[q, sub], dx_recv.at[q, sub]
+            )
+        product(shard, 1 - rep)
+        join_cores(shard, rep)
+        join_sides(before)
+    last = shard_order[3]
+    join_cores(last, 1 - rep)
+    join_sides(last)
+    conclude(partner)
+    conclude(jnp.where(outer, same, fs))
+    conclude(far)
+    conclude(jnp.where(outer, fs, same))
+
+    for copy in sent:
+        copy.wait_send()
+    for part in range(TOKEN_PARTS):
+        piece = token_part(0, tp, part)
+        remote(piece, piece, rz_send.at[part], rz_recv.at[part], {"fs": partner}).wait_send()
+    for shard in range(4):
+        y_copy(shard).wait_send()
+
+    @pl.loop(0, chunks)
+    def _(j):
+        for copy in chunk_copies(j):
+            copy.wait_send()
+
+        @pl.when(j >= ahead)
+        def _():
+            for q, f in enumerate(sources):
+                piece = chunk_target(j, f, rep)
+                remote(piece, piece, gx_send.at[j, q], gx_recv.at[j, q], mirror).wait_send()
+
+
+def pair_shards(
+    residual,
+    mixer_gain,
+    pool_weight,
+    pool_scale,
+    channel_gain,
+    gate_weight,
+    up_weight,
+    gate_scale,
+    up_scale,
+    gate_taps,
+    up_taps,
+    down_weight,
+    down_scale,
+):
+    _, length, groups, local = residual.shape
+    channels = local * 4
+    width = groups * channels
+    rows, hidden_width = gate_weight.shape
+    half = hidden_width // 2
+    chunks = half // 128
+    half_columns = down_weight.shape[1] // 2
+    vmem = pl.BlockSpec(memory_space=pltpu.VMEM)
+    anywhere = pl.BlockSpec(memory_space=pl.ANY)
+    dma = pltpu.SemaphoreType.DMA
+    pairs = [
+        (3, 3),
+        (2, 3),
+        (3,),
+        (3,),
+        (3,),
+        (TOKEN_PARTS,),
+        (2, TOKEN_PARTS),
+        (4, TOKEN_PARTS),
+        (chunks, 3),
+        (chunks, 3),
+        (3, PIECES),
+        (3, PIECES),
+        (4, 2),
+        (4,),
+        (4,),
+    ]
+    out = pl.pallas_call(
+        pair_kernel,
+        out_shape=jax.ShapeDtypeStruct((length, groups * local), BF16),
+        in_specs=[anywhere] + [vmem] * 8 + [anywhere] * 4,
+        out_specs=vmem,
+        scratch_shapes=[
+            pltpu.VMEM((2, rows, half), F32),
+            pltpu.VMEM((2, rows // 2, half), F32),
+            pltpu.VMEM((half, 2 * half_columns), F32),
+            pltpu.VMEM((half, half_columns), F32),
+            pltpu.VMEM(pool_weight.shape, F32),
+            pltpu.VMEM((2, 4, length, groups * local), BF16),
+            pltpu.VMEM((4, 3, groups, local), F32),
+            pltpu.VMEM((4, 2) + gate_scale.shape, F32),
+            pltpu.VMEM(pool_weight.shape, BF16),
+            pltpu.VMEM((groups, channels, channels), BF16),
+            pltpu.VMEM((chunks, 4, rows, 256), BF16),
+            pltpu.VMEM((chunks, rows // 2, 256), BF16),
+            pltpu.VMEM((4, 2, half, half_columns), BF16),
+            pltpu.VMEM((half, half_columns), BF16),
+            pltpu.VMEM((length, channels), BF16),
+            pltpu.VMEM((length, channels), BF16),
+            pltpu.VMEM((2 * length, width), BF16),
+            pltpu.VMEM((length, groups * local), BF16),
+            pltpu.VMEM((2 * length, half), BF16),
+            pltpu.VMEM((4, 2, 2 * length, local), F32),
+            pltpu.VMEM((4, 2, 2 * length, local), BF16),
+            pltpu.VMEM((4, 2, 2 * length, local), BF16),
+            pltpu.VMEM((4, 2 * length, local), BF16),
+            pltpu.VMEM((4, 2 * length, local), BF16),
+            pltpu.VMEM((4, length, local), BF16),
+            pltpu.VMEM((4, length, local), BF16),
+        ]
+        + [dma(shape) for shape in pairs for _ in range(2)]
+        + [dma((9,))],
+        compiler_params=pltpu.CompilerParams(
+            collective_id=0, has_side_effects=True, vmem_limit_bytes=VMEM_BYTES
+        ),
+    )(
+        residual.reshape(length, groups * local),
+        mixer_gain,
+        pool_scale,
+        channel_gain,
+        down_scale,
+        gate_scale,
+        up_scale,
+        gate_taps,
+        up_taps,
+        pool_weight,
+        gate_weight,
+        up_weight,
+        down_weight,
+    )
+    return out.reshape(1, length, groups, local)
+
+
+def paired(sizes, residual, gate_weight, down_weight):
+    _, length, groups, local = residual
+    return (
+        sizes == (2, 4, 4)
+        and residual[0] == 1
+        and local == 128
+        and length % BAND == 0
+        and groups == len(WINDOWS)
+        and down_weight[1] == 4 * local
+        and gate_weight[0] * 4 == groups * local * 4
+        and gate_weight[1] % 512 == 0
+    )
+
+
 def shards(
     sizes,
     residual,
@@ -483,6 +1111,22 @@
     down_weight,
     down_scale,
 ):
+    if paired(sizes, residual.shape, gate_weight.shape, down_weight.shape):
+        return pair_shards(
+            residual,
+            mixer_gain,
+            pool_weight,
+            pool_scale,
+            channel_gain,
+            gate_weight,
+            up_weight,
+            gate_scale,
+            up_scale,
+            gate_taps,
+            up_taps,
+            down_weight,
+            down_scale,
+        )
     n_rep, n_fs, n_tp = sizes
     _, length, groups, local = residual.shape
     channels = local * n_tp

time: 216 us -> 168 us (0.78)
  Pallas kernels: 199 us -> 161 us
  other arithmetic: 10.1 us -> 0 us
    pallas_call x1, Pallas kernels: 199 us -> 161 us  [pair_shards(): pl.pallas_call(pair_kernel, out_shape=jax.ShapeDtypeStruct((length, group...]
    convert_element_type x4 -> x0, other arithmetic: 7.53 us -> none  [the longest x1 3.22 us: shards(): gate_weight.astype(BF16)]
where the time goes in v1:
time: 168 us; the launch traced here: 166 us
  Pallas kernels  161 us (96%)
  local copies, waits for them, and re-layouts  4.59 us (3%)
    pallas_call x1, Pallas kernels, pair_shards(): pl.pallas_call(pair_kernel, out_shape=jax.ShapeDtypeStruct((length, group...  161 us

profile of v1, /device:TPU:0, one launch (start us, length us, event | category | flops | bytes accessed | tf_op | source)
XLA Modules:
  0.0 165.6 jit_solution(15320215826318167382)
XLA Ops:
  0.0 2.1 %copy.16 = bf16[96,8,4,128]{3,1,2,0:T(8,128)(2,1)} copy(bf16[96,8,4,128]{3,2,1,0:T(4,128)(2,1)} %bitcast.6) | data formatting | bytes 1572864
  2.1 161.0 %shard_map.127 = bf16[768,512]{1,0:T(8,128)(2,1)} custom-call(bf16[768,512]{1,0:T(8,128)(2,1)} %bitcast.5, f32[4,128]{1,0:T(4,128)} %mixer_gain.1, f32[4,128]{1,0:T(4,128)} %pool_scale.1, f32[4,128]{1,0:T(4,128)} %channel_gain.1, f32[4,128]{1,0:T(4,128)} %down_scale.1, f32[1,384]{1,0:T(1,128)} %gate_scale.1, f32[1,384]{1,0:T(1,128)} %up_scale.1, ...), custom_call_target="tpu_custom_call" | custom-call | tf_op jit(solution)/shard_map/pallas_call | solution.py:1028
  163.1 2.4 %reshape.7 = bf16[1,768,4,128]{3,2,1,0:T(4,128)(2,1)} reshape(bf16[768,512]{1,0:T(8,128)(2,1)} %shard_map.127) | data formatting | bytes 1572864 | tf_op jit(solution)/shard_map/reshape | solution.py:1081

commit v2 on v1

--- a/solution.py
+++ b/solution.py
@@ -566,6 +566,7 @@
     same, far, partner = lax.rem(fs + 2, 4), 3 - fs, fs + 1 - 2 * member
     sources = (same, far, partner)
     outer = (fs == 0) | (fs == 3)
+    inner = jnp.logical_not(outer)
 
     sent = []
 
@@ -637,14 +638,17 @@
             aligned(tp * local, local),
         ]
 
-    for q, f in enumerate(sources):
-        start(
+    def pool_copy_to(q):
+        return remote(
             pool_near.at[pl.ds(rep * (groups // 2), groups // 2)],
             pool_part(fs, rep),
             pz_send.at[q],
             pz_recv.at[q],
-            {"fs": f},
+            {"fs": sources[q]},
         )
+
+    for q in (2, 1, 0):
+        pool_copy_to(q).start()
     for part in range(TOKEN_PARTS):
         piece = token_part(0, tp, part)
         start(piece, piece, ry_send.at[0, part], ry_recv.at[0, part], across)
@@ -663,18 +667,36 @@
         8,
     )
 
+    late, late_kind = jnp.where(outer, far, same), jnp.where(outer, 1, 0)
+
     def chunk_target(j, shard, half):
         return weights.at[j, shard, aligned(half * half_rows, half_rows)]
 
-    def chunk_copies(j):
+    def chunk_copy(j, q):
         target = chunk_target(j, fs, rep)
-        return [
-            remote(source, target, gz_send.at[j, q], gz_recv.at[j, q], {"fs": f})
-            for q, (source, f) in enumerate(
-                ((target, same), (other.at[j], far), (other.at[j], partner))
-            )
-        ]
-
+        source = target if q == 0 else other.at[j]
+        return remote(source, target, gz_send.at[j, q], gz_recv.at[j, q], {"fs": sources[q]})
+
+    def down_part(shard, half, sub):
+        span = half_hidden // PIECES
+        return down_full.at[shard, half, pl.ds(sub * span, span)]
+
+    def down_copy(q, sub):
+        span = half_hidden // PIECES
+        target = down_part(fs, rep, sub)
+        source = target if q == 0 else down_other.at[pl.ds(sub * span, span)]
+        return remote(source, target, dz_send.at[q, sub], dz_recv.at[q, sub], {"fs": sources[q]})
+
+    def token_copy(part):
+        return remote(
+            token_part(0, tp, part),
+            token_part(1, tp, part),
+            rz_send.at[part],
+            rz_recv.at[part],
+            {"fs": partner},
+        )
+
+    before_tokens = 2
     for load in loads:
         load.wait()
 
@@ -685,19 +707,13 @@
             lanes = slice(at * 128, (at + 1) * 128)
             weights[j, fs, :, lanes] = stage_own[at, :, columns].astype(BF16)
             other[j, :, lanes] = stage_other[at, :, columns].astype(BF16)
-        for copy in chunk_copies(j):
-            copy.start()
-
-        @pl.when(j == 0)
+        chunk_copy(j, 2).start()
+        pl.when(inner)(chunk_copy(j, 1).start)
+
+        @pl.when(j == before_tokens - 1)
         def _():
             for part in range(TOKEN_PARTS):
-                remote(
-                    token_part(0, tp, part),
-                    token_part(1, tp, part),
-                    rz_send.at[part],
-                    rz_recv.at[part],
-                    {"fs": partner},
-                ).start()
+                token_copy(part).start()
 
     for load in load_down:
         load.wait()
@@ -706,29 +722,43 @@
             :, half * half_columns : (half + 1) * half_columns
         ].astype(BF16)
     down_other[...] = stage_down_other[...].astype(BF16)
-
-    def down_part(shard, half, sub):
-        span = half_hidden // PIECES
-        return down_full.at[shard, half, pl.ds(sub * span, span)]
-
-    for q, f in enumerate(sources):
+    for sub in range(PIECES):
+        down_copy(2, sub).start()
+
+    @pl.when(inner)
+    def _():
         for sub in range(PIECES):
-            span = half_hidden // PIECES
-            source = (
-                down_part(fs, rep, sub) if q == 0 else down_other.at[pl.ds(sub * span, span)]
-            )
-            start(
-                source,
-                down_part(fs, rep, sub),
-                dz_send.at[q, sub],
-                dz_recv.at[q, sub],
-                {"fs": f},
-            )
+            down_copy(1, sub).start()
+
+        @pl.loop(0, chunks)
+        def _(j):
+            chunk_copy(j, 0).start()
+
+        for sub in range(PIECES):
+            down_copy(0, sub).start()
 
     def landed(ref, send, recv):
         remote(ref, ref, send, recv, mirror).wait_recv()
 
-    for q, f in enumerate(sources):
+    def chunk_onward(j, q, shard):
+        piece = chunk_target(j, shard, rep)
+        return remote(piece, piece, gx_send.at[j, q], gx_recv.at[j, q], mirror)
+
+    def forward_chunk(j, q, shard):
+        piece = chunk_target(j, shard, rep)
+        landed(piece, gz_send.at[j, q], gz_recv.at[j, q])
+        chunk_onward(j, q, shard).start()
+
+    def down_onward(q, shard, sub):
+        piece = down_part(shard, rep, sub)
+        return remote(piece, piece, dx_send.at[q, sub], dx_recv.at[q, sub], mirror)
+
+    def forward_down(q, shard, subs=range(PIECES)):
+        for sub in subs:
+            landed(down_part(shard, rep, sub), dz_send.at[q, sub], dz_recv.at[q, sub])
+            down_onward(q, shard, sub).start()
+
+    for q, f in ((2, partner), (1, far), (0, same)):
         piece = pool_part(f, rep)
         landed(piece, pz_send.at[q], pz_recv.at[q])
         start(piece, piece, px_send.at[q], px_recv.at[q], mirror)
@@ -743,26 +773,43 @@
     start(slab, slab, pt_send.at[1], pt_recv.at[1], across)
     start(slab, slab, pt_send.at[0], pt_recv.at[0], sibling)
 
-    def forward_chunk(j, do_start):
-        for q, f in enumerate(sources):
-            piece = chunk_target(j, f, rep)
-            landed(piece, gz_send.at[j, q], gz_recv.at[j, q])
-            do_start(piece, piece, gx_send.at[j, q], gx_recv.at[j, q], mirror)
-
     t_sibling, t_across, t_diagonal = sibling["tp"], across["tp"], diagonal["tp"]
-    for part in range(TOKEN_PARTS):
+
+    def own_onward(part):
         piece = token_part(0, t_across, part)
         landed(piece, ry_send.at[0, part], ry_recv.at[0, part])
         start(piece, piece, rs_send.at[1, part], rs_recv.at[1, part], sibling)
-    forward_chunk(0, start)
-    for part in range(TOKEN_PARTS):
+
+    def partner_onward(part):
         piece = token_part(1, tp, part)
         landed(piece, rz_send.at[part], rz_recv.at[part])
         start(piece, piece, ry_send.at[1, part], ry_recv.at[1, part], across)
         start(piece, piece, rs_send.at[2, part], rs_recv.at[2, part], sibling)
+
+    for j in range(before_tokens):
+        forward_chunk(j, 2, partner)
+        pl.when(inner)(functools.partial(forward_chunk, j, 1, far))
+    own_onward(0)
+
+    @pl.when(inner)
+    def _():
+        for j in range(before_tokens, chunks - 2):
+            forward_chunk(j, 1, far)
+
+    own_onward(1)
+    partner_onward(0)
+
+    @pl.when(inner)
+    def _():
+        for j in range(chunks - 2, chunks):
+            forward_chunk(j, 1, far)
+
+    partner_onward(1)
+    pl.when(inner)(functools.partial(forward_down, 1, far))
     slab = pool_slab(t_across)
     landed(slab, pt_send.at[1], pt_recv.at[1])
     start(slab, slab, pt_send.at[2], pt_recv.at[2], sibling)
+    pl.when(outer)(functools.partial(forward_chunk, 0, 0, same))
     for part in range(TOKEN_PARTS):
         landed(token_part(0, t_sibling, part), rs_send.at[0, part], rs_recv.at[0, part])
         landed(token_part(0, t_diagonal, part), rs_send.at[1, part], rs_recv.at[1, part])
@@ -831,7 +878,27 @@
                 ).astype(BF16)
 
     mix(0)
-    forward_chunk(1, start)
+
+    @pl.when(outer)
+    def _():
+        for j in range(1, chunks):
+            forward_chunk(j, 0, same)
+
+        @pl.loop(0, chunks)
+        def _(j):
+            chunk_copy(j, 0).start()
+            chunk_copy(j, 1).start()
+
+        for sub in range(PIECES):
+            down_copy(0, sub).start()
+            down_copy(1, sub).start()
+
+    @pl.when(inner)
+    def _():
+        for j in range(before_tokens, chunks):
+            forward_chunk(j, 2, partner)
+        forward_down(2, partner)
+
     for part in range(TOKEN_PARTS):
         piece = token_part(1, t_across, part)
         landed(piece, ry_send.at[1, part], ry_recv.at[1, part])
@@ -839,21 +906,14 @@
     for part in range(TOKEN_PARTS):
         landed(token_part(1, t_sibling, part), rs_send.at[2, part], rs_recv.at[2, part])
         landed(token_part(1, t_diagonal, part), rs_send.at[3, part], rs_recv.at[3, part])
-    forward_chunk(2, start)
     mix(1)
-    forward_chunk(3, start)
     for at in range(2):
         for q, f in enumerate(sources):
             landed(scales_all.at[f, at], scale_send.at[at, q], scale_recv.at[at, q])
 
-    ahead = 4
     thirds = scales_all.shape[3] // 128
 
-    def start_only(*parts):
-        remote(*parts).start()
-
-    @pl.loop(0, chunks)
-    def _(j):
+    def expand(j):
         for q, f in enumerate(sources):
             landed(chunk_target(j, f, 1 - rep), gx_send.at[j, q], gx_recv.at[j, q])
         here = aligned(member * half_hidden + j * 128, 128)
@@ -872,53 +932,73 @@
             silu = conv_gate / (1.0 + jnp.exp(-conv_gate))
             hidden[span, aligned(j * 128, 128)] = (silu * conv_up).astype(BF16)
 
-        @pl.when(j + ahead < chunks)
+    @pl.loop(0, chunks + 2)
+    def _(j):
+        @pl.when(outer & (j < chunks - before_tokens))
         def _():
-            forward_chunk(j + ahead, start_only)
-
-    kinds = (jnp.where(outer, 2, 1), jnp.int32(0), jnp.where(outer, 1, 2))
-    shard_order = (
-        fs,
-        jnp.where(outer, partner, far),
-        same,
-        jnp.where(outer, far, partner),
-    )
+            forward_chunk(j + before_tokens, 2, partner)
+
+        @pl.when(j < chunks)
+        def _():
+            forward_chunk(j, late_kind, late)
+
+        @pl.when(outer & (j == chunks))
+        def _():
+            forward_down(2, partner)
+
+        @pl.when(j > 1)
+        def _():
+            expand(j - 2)
+
+    def core_copy(shard, half, slot):
+        return remote(
+            give.at[shard, half, slot],
+            got.at[shard, half, slot],
+            core_send.at[shard, half, slot],
+            core_recv.at[shard, half, slot],
+            sibling,
+        )
 
     def product(shard, half):
         for slot in (1, 0):
             span = slice(slot * length, (slot + 1) * length)
             made = jnp.dot(hidden[span], down_full[shard, half], preferred_element_type=F32)
             low, high = made[:, :local], made[:, local:]
-            keep[shard, half, span] = jnp.where(core == 0, low, high)
-            give[shard, half, span] = jnp.where(core == 0, high, low).astype(BF16)
-        start(
-            give.at[shard, half],
-            got.at[shard, half],
-            core_send.at[shard, half],
-            core_recv.at[shard, half],
-            sibling,
+            keep[shard, half, slot] = jnp.where(core == 0, low, high)
+            give[shard, half, slot] = jnp.where(core == 0, high, low).astype(BF16)
+            core_copy(shard, half, slot).start()
+
+    def y_copy(shard, slot):
+        return remote(
+            y_out.at[shard, slot],
+            y_in.at[shard, slot],
+            y_send.at[shard, slot],
+            y_recv.at[shard, slot],
+            across,
         )
 
-    def y_copy(shard):
-        return remote(y_out.at[shard], y_in.at[shard], y_send.at[shard], y_recv.at[shard], across)
+    def arrived_x(q, shard):
+        for sub in range(PIECES):
+            landed(down_part(shard, 1 - rep, sub), dx_send.at[q, sub], dx_recv.at[q, sub])
 
     def join_cores(shard, half):
-        landed(got.at[shard, half], core_send.at[shard, half], core_recv.at[shard, half])
-        total = keep[shard, half] + got[shard, half].astype(F32)
-
-        @pl.when(half == side)
-        def _():
-            keep[shard, half] = total
-
-        @pl.when(half != side)
-        def _():
-            y_out[shard] = total.astype(BF16)
-            y_copy(shard).start()
+        for slot in (1, 0):
+            core_copy(shard, half, slot).wait_recv()
+            total = keep[shard, half, slot] + got[shard, half, slot].astype(F32)
+
+            @pl.when(half == side)
+            def _():
+                keep[shard, half, slot] = total
+
+            @pl.when(half != side)
+            def _():
+                y_out[shard, slot] = total.astype(BF16)
+                y_copy(shard, slot).start()
 
     def join_sides(shard):
-        landed(y_in.at[shard], y_send.at[shard], y_recv.at[shard])
-        total = keep[shard, side] + y_in[shard].astype(F32)
-        z_out[shard] = total[length:].astype(BF16)
+        y_copy(shard, 1).wait_recv()
+        total = keep[shard, side, 1] + y_in[shard, 1].astype(F32)
+        z_out[shard] = total.astype(BF16)
         start(
             z_out.at[shard],
             z_in.at[shard],
@@ -926,61 +1006,79 @@
             z_recv.at[shard],
             {"fs": partner},
         )
-        keep[shard, side, :length] = total[:length]
 
     def conclude(shard):
+        y_copy(shard, 0).wait_recv()
+        total = keep[shard, side, 0] + y_in[shard, 0].astype(F32)
         landed(z_in.at[shard], z_send.at[shard], z_recv.at[shard])
         columns = aligned(shard * local, local)
-        total = keep[shard, side, :length] + z_in[shard].astype(F32)
+        total = total + z_in[shard].astype(F32)
         out[:, columns] = (
             total * down_scale[pl.ds(shard, 1), :] + middle[:, columns].astype(F32)
         ).astype(BF16)
 
+    early, early_kind = jnp.where(outer, partner, far), jnp.where(outer, 2, 1)
+    later, later_kind = jnp.where(outer, far, partner), jnp.where(outer, 1, 2)
+
+    def later_products():
+        product(later, rep)
+        arrived_x(later_kind, later)
+        product(later, 1 - rep)
+
     product(fs, rep)
     product(fs, 1 - rep)
     join_cores(fs, rep)
-    for k in range(1, 4):
-        shard, q = shard_order[k], kinds[k - 1]
-        before = shard_order[k - 1]
-        for sub in range(PIECES):
-            piece = down_part(shard, rep, sub)
-            landed(piece, dz_send.at[q, sub], dz_recv.at[q, sub])
-            start(piece, piece, dx_send.at[q, sub], dx_recv.at[q, sub], mirror)
-        product(shard, rep)
-        join_cores(before, 1 - rep)
-        for sub in range(PIECES):
-            landed(
-                down_part(shard, 1 - rep, sub), dx_send.at[q, sub], dx_recv.at[q, sub]
-            )
-        product(shard, 1 - rep)
-        join_cores(shard, rep)
-        join_sides(before)
-    last = shard_order[3]
-    join_cores(last, 1 - rep)
-    join_sides(last)
+    forward_down(late_kind, late, (0,))
+    product(early, rep)
+    join_cores(fs, 1 - rep)
+    forward_down(late_kind, late, (1,))
+    arrived_x(early_kind, early)
+    product(early, 1 - rep)
+    join_cores(early, rep)
+    forward_down(late_kind, late, (2,))
+    pl.when(inner)(later_products)
+    join_cores(early, 1 - rep)
+    forward_down(late_kind, late, (3,))
+    join_sides(fs)
+    pl.when(outer)(functools.partial(forward_down, 0, same, (0, 1)))
+    pl.when(outer)(later_products)
+    join_cores(later, rep)
+    join_cores(later, 1 - rep)
+    pl.when(outer)(functools.partial(forward_down, 0, same, (2, 3)))
+    product(same, rep)
+    join_sides(early)
+    arrived_x(0, same)
+    product(same, 1 - rep)
+    join_cores(same, rep)
+    join_cores(same, 1 - rep)
+    join_sides(later)
+    join_sides(same)
     conclude(partner)
     conclude(jnp.where(outer, same, fs))
+    conclude(jnp.where(outer, fs, same))
     conclude(far)
-    conclude(jnp.where(outer, fs, same))
 
     for copy in sent:
         copy.wait_send()
+    for q in range(3):
+        pool_copy_to(q).wait_send()
     for part in range(TOKEN_PARTS):
-        piece = token_part(0, tp, part)
-        remote(piece, piece, rz_send.at[part], rz_recv.at[part], {"fs": partner}).wait_send()
+        token_copy(part).wait_send()
     for shard in range(4):
-        y_copy(shard).wait_send()
+        for slot in range(2):
+            y_copy(shard, slot).wait_send()
+            for half in range(2):
+                core_copy(shard, half, slot).wait_send()
+    for q, f in enumerate(sources):
+        for sub in range(PIECES):
+            down_copy(q, sub).wait_send()
+            down_onward(q, f, sub).wait_send()
 
     @pl.loop(0, chunks)
     def _(j):
-        for copy in chunk_copies(j):
-            copy.wait_send()
-
-        @pl.when(j >= ahead)
-        def _():
-            for q, f in enumerate(sources):
-                piece = chunk_target(j, f, rep)
-                remote(piece, piece, gx_send.at[j, q], gx_recv.at[j, q], mirror).wait_send()
+        for q, f in enumerate(sources):
+            chunk_copy(j, q).wait_send()
+            chunk_onward(j, q, f).wait_send()
 
 
 def pair_shards(
@@ -1021,8 +1119,8 @@
         (chunks, 3),
         (3, PIECES),
         (3, PIECES),
+        (4, 2, 2),
         (4, 2),
-        (4,),
         (4,),
     ]
     out = pl.pallas_call(
@@ -1050,11 +1148,11 @@
             pltpu.VMEM((2 * length, width), BF16),
             pltpu.VMEM((length, groups * local), BF16),
             pltpu.VMEM((2 * length, half), BF16),
-            pltpu.VMEM((4, 2, 2 * length, local), F32),
-            pltpu.VMEM((4, 2, 2 * length, local), BF16),
-            pltpu.VMEM((4, 2, 2 * length, local), BF16),
-            pltpu.VMEM((4, 2 * length, local), BF16),
-            pltpu.VMEM((4, 2 * length, local), BF16),
+            pltpu.VMEM((4, 2, 2, length, local), F32),
+            pltpu.VMEM((4, 2, 2, length, local), BF16),
+            pltpu.VMEM((4, 2, 2, length, local), BF16),
+            pltpu.VMEM((4, 2, length, local), BF16),
+            pltpu.VMEM((4, 2, length, local), BF16),
             pltpu.VMEM((4, length, local), BF16),
             pltpu.VMEM((4, length, local), BF16),
         ]

time: 168 us -> 150 us (0.89)
  Pallas kernels: 161 us -> 144 us
    pallas_call x1, Pallas kernels: 161 us -> 144 us  [pair_shards(): pl.pallas_call(pair_kernel, out_shape=jax.ShapeDtypeStruct((length, group...]
where the time goes in v2:
time: 150 us; the launch traced here: 148 us
  Pallas kernels  144 us (96%)
  local copies, waits for them, and re-layouts  4.59 us (3%)
    pallas_call x1, Pallas kernels, pair_shards(): pl.pallas_call(pair_kernel, out_shape=jax.ShapeDtypeStruct((length, group...  144 us

profile of v2, /device:TPU:0, one launch (start us, length us, event | category | flops | bytes accessed | tf_op | source)
XLA Modules:
  0.0 148.3 jit_solution(3872010801584418292)
XLA Ops:
  0.0 2.1 %copy.16 = bf16[96,8,4,128]{3,1,2,0:T(8,128)(2,1)} copy(bf16[96,8,4,128]{3,2,1,0:T(4,128)(2,1)} %bitcast.6) | data formatting | bytes 1572864
  2.1 143.7 %shard_map.127 = bf16[768,512]{1,0:T(8,128)(2,1)} custom-call(bf16[768,512]{1,0:T(8,128)(2,1)} %bitcast.5, f32[4,128]{1,0:T(4,128)} %mixer_gain.1, f32[4,128]{1,0:T(4,128)} %pool_scale.1, f32[4,128]{1,0:T(4,128)} %channel_gain.1, f32[4,128]{1,0:T(4,128)} %down_scale.1, f32[1,384]{1,0:T(1,128)} %gate_scale.1, f32[1,384]{1,0:T(1,128)} %up_scale.1, ...), custom_call_target="tpu_custom_call" | custom-call | tf_op jit(solution)/shard_map/pallas_call | solution.py:1126
  145.9 2.4 %reshape.7 = bf16[1,768,4,128]{3,2,1,0:T(4,128)(2,1)} reshape(bf16[768,512]{1,0:T(8,128)(2,1)} %shard_map.127) | data formatting | bytes 1572864 | tf_op jit(solution)/shard_map/reshape | solution.py:1179

commit v3 on v2

--- a/solution.py
+++ b/solution.py
@@ -696,7 +696,8 @@
             {"fs": partner},
         )
 
-    before_tokens = 2
+    for part in range(TOKEN_PARTS):
+        token_copy(part).start()
     for load in loads:
         load.wait()
 
@@ -710,10 +711,11 @@
         chunk_copy(j, 2).start()
         pl.when(inner)(chunk_copy(j, 1).start)
 
-        @pl.when(j == before_tokens - 1)
-        def _():
-            for part in range(TOKEN_PARTS):
-                token_copy(part).start()
+    @pl.when(inner)
+    def _():
+        @pl.loop(0, chunks)
+        def _(j):
+            chunk_copy(j, 0).start()
 
     for load in load_down:
         load.wait()
@@ -722,20 +724,12 @@
             :, half * half_columns : (half + 1) * half_columns
         ].astype(BF16)
     down_other[...] = stage_down_other[...].astype(BF16)
-    for sub in range(PIECES):
-        down_copy(2, sub).start()
 
     @pl.when(inner)
     def _():
-        for sub in range(PIECES):
-            down_copy(1, sub).start()
-
-        @pl.loop(0, chunks)
-        def _(j):
-            chunk_copy(j, 0).start()
-
-        for sub in range(PIECES):
-            down_copy(0, sub).start()
+        for q in (2, 0, 1):
+            for sub in range(PIECES):
+                down_copy(q, sub).start()
 
     def landed(ref, send, recv):
         remote(ref, ref, send, recv, mirror).wait_recv()
@@ -786,30 +780,25 @@
         start(piece, piece, ry_send.at[1, part], ry_recv.at[1, part], across)
         start(piece, piece, rs_send.at[2, part], rs_recv.at[2, part], sibling)
 
-    for j in range(before_tokens):
-        forward_chunk(j, 2, partner)
-        pl.when(inner)(functools.partial(forward_chunk, j, 1, far))
+    def forward_chunks(kind, shard, low, high):
+        for j in range(low, high):
+            forward_chunk(j, kind, shard)
+
+    third = chunks // 3
     own_onward(0)
-
-    @pl.when(inner)
-    def _():
-        for j in range(before_tokens, chunks - 2):
-            forward_chunk(j, 1, far)
-
+    pl.when(inner)(functools.partial(forward_chunks, 1, far, 0, third))
+    partner_onward(0)
     own_onward(1)
-    partner_onward(0)
-
-    @pl.when(inner)
-    def _():
-        for j in range(chunks - 2, chunks):
-            forward_chunk(j, 1, far)
-
+    pl.when(inner)(functools.partial(forward_chunks, 1, far, third, chunks - 1))
     partner_onward(1)
-    pl.when(inner)(functools.partial(forward_down, 1, far))
+    pl.when(inner)(functools.partial(forward_chunks, 1, far, chunks - 1, chunks))
+    second_kind, second = jnp.where(outer, 0, 2), jnp.where(outer, same, partner)
+    forward_chunks(second_kind, second, 0, 2)
     slab = pool_slab(t_across)
     landed(slab, pt_send.at[1], pt_recv.at[1])
     start(slab, slab, pt_send.at[2], pt_recv.at[2], sibling)
-    pl.when(outer)(functools.partial(forward_chunk, 0, 0, same))
+    forward_chunks(second_kind, second, 2, chunks // 2)
+
     for part in range(TOKEN_PARTS):
         landed(token_part(0, t_sibling, part), rs_send.at[0, part], rs_recv.at[0, part])
         landed(token_part(0, t_diagonal, part), rs_send.at[1, part], rs_recv.at[1, part])
@@ -826,7 +815,7 @@
         - lax.broadcasted_iota(jnp.int32, (BAND, 2 * BAND), 1)
     )
 
-    def mix(slot):
+    def mix(slot, between):
         span = slice(slot * length, (slot + 1) * length)
         square = jnp.zeros((length, local), F32)
         for t in range(4):
@@ -836,6 +825,8 @@
         factor = lax.rsqrt(jnp.sum(square, axis=1, keepdims=True) / width + EPSILON)
         square = jnp.zeros((length, local), F32)
         for g in range(groups):
+            if g == groups // 2:
+                between()
             part = slice(g * local, (g + 1) * local)
             for t in range(4):
                 values = tokens[slot, t, :, part].astype(F32)
@@ -877,36 +868,34 @@
                     inputs[span, columns].astype(F32) * factor * small_all[t, 2, g : g + 1]
                 ).astype(BF16)
 
-    mix(0)
+    mix(0, functools.partial(forward_chunks, second_kind, second, chunks // 2, chunks // 2 + 1))
+    forward_chunks(second_kind, second, chunks // 2 + 1, chunks)
 
     @pl.when(outer)
     def _():
-        for j in range(1, chunks):
-            forward_chunk(j, 0, same)
-
         @pl.loop(0, chunks)
         def _(j):
+            chunk_copy(j, 1).start()
             chunk_copy(j, 0).start()
-            chunk_copy(j, 1).start()
 
         for sub in range(PIECES):
-            down_copy(0, sub).start()
-            down_copy(1, sub).start()
-
-    @pl.when(inner)
-    def _():
-        for j in range(before_tokens, chunks):
-            forward_chunk(j, 2, partner)
-        forward_down(2, partner)
+            down_copy(2, sub).start()
 
     for part in range(TOKEN_PARTS):
         piece = token_part(1, t_across, part)
         landed(piece, ry_send.at[1, part], ry_recv.at[1, part])
         start(piece, piece, rs_send.at[3, part], rs_recv.at[3, part], sibling)
+    pl.when(outer)(functools.partial(forward_chunk, 0, 1, far))
     for part in range(TOKEN_PARTS):
         landed(token_part(1, t_sibling, part), rs_send.at[2, part], rs_recv.at[2, part])
         landed(token_part(1, t_diagonal, part), rs_send.at[3, part], rs_recv.at[3, part])
-    mix(1)
+
+    def forward_late(j):
+        forward_chunk(j, late_kind, late)
+        pl.when(outer)(functools.partial(forward_chunk, j, 2, partner))
+
+    forward_chunk(0, jnp.where(outer, 2, 0), jnp.where(outer, partner, same))
+    mix(1, functools.partial(forward_late, 1))
     for at in range(2):
         for q, f in enumerate(sources):
             landed(scales_all.at[f, at], scale_send.at[at, q], scale_recv.at[at, q])
@@ -932,23 +921,20 @@
             silu = conv_gate / (1.0 + jnp.exp(-conv_gate))
             hidden[span, aligned(j * 128, 128)] = (silu * conv_up).astype(BF16)
 
-    @pl.loop(0, chunks + 2)
+    @pl.loop(0, chunks)
     def _(j):
-        @pl.when(outer & (j < chunks - before_tokens))
+        expand(j)
+
+        @pl.when(j < chunks - 2)
         def _():
-            forward_chunk(j + before_tokens, 2, partner)
-
-        @pl.when(j < chunks)
+            forward_late(j + 2)
+
+        @pl.when(outer & (j == chunks - 2))
         def _():
-            forward_chunk(j, late_kind, late)
-
-        @pl.when(outer & (j == chunks))
-        def _():
-            forward_down(2, partner)
-
-        @pl.when(j > 1)
-        def _():
-            expand(j - 2)
+            forward_down(0, same)
+            for sub in range(PIECES):
+                down_copy(1, sub).start()
+                down_copy(0, sub).start()
 
     def core_copy(shard, half, slot):
         return remote(
@@ -1017,46 +1003,47 @@
             total * down_scale[pl.ds(shard, 1), :] + middle[:, columns].astype(F32)
         ).astype(BF16)
 
-    early, early_kind = jnp.where(outer, partner, far), jnp.where(outer, 2, 1)
-    later, later_kind = jnp.where(outer, far, partner), jnp.where(outer, 1, 2)
-
-    def later_products():
-        product(later, rep)
-        arrived_x(later_kind, later)
-        product(later, 1 - rep)
+    early, early_kind = jnp.where(outer, same, partner), jnp.where(outer, 0, 2)
+    later, later_kind = jnp.where(outer, partner, same), jnp.where(outer, 2, 0)
+
+    def pass_on(sub):
+        pl.when(outer)(functools.partial(forward_down, 2, partner, (sub,)))
+        forward_down(late_kind, late, (sub,))
 
     product(fs, rep)
     product(fs, 1 - rep)
     join_cores(fs, rep)
-    forward_down(late_kind, late, (0,))
+    pl.when(inner)(functools.partial(forward_down, 2, partner))
+    join_cores(fs, 1 - rep)
     product(early, rep)
-    join_cores(fs, 1 - rep)
-    forward_down(late_kind, late, (1,))
+    pass_on(0)
     arrived_x(early_kind, early)
     product(early, 1 - rep)
     join_cores(early, rep)
-    forward_down(late_kind, late, (2,))
-    pl.when(inner)(later_products)
+    pass_on(1)
     join_cores(early, 1 - rep)
-    forward_down(late_kind, late, (3,))
+    pass_on(2)
     join_sides(fs)
-    pl.when(outer)(functools.partial(forward_down, 0, same, (0, 1)))
-    pl.when(outer)(later_products)
+    pass_on(3)
+    product(later, rep)
+    pl.when(inner)(functools.partial(forward_down, 1, far, (0, 1)))
+    arrived_x(later_kind, later)
+    product(later, 1 - rep)
     join_cores(later, rep)
+    pl.when(inner)(functools.partial(forward_down, 1, far, (2, 3)))
     join_cores(later, 1 - rep)
-    pl.when(outer)(functools.partial(forward_down, 0, same, (2, 3)))
-    product(same, rep)
     join_sides(early)
-    arrived_x(0, same)
-    product(same, 1 - rep)
-    join_cores(same, rep)
-    join_cores(same, 1 - rep)
+    product(far, rep)
+    arrived_x(1, far)
+    product(far, 1 - rep)
+    join_cores(far, rep)
+    join_cores(far, 1 - rep)
     join_sides(later)
-    join_sides(same)
+    join_sides(far)
     conclude(partner)
-    conclude(jnp.where(outer, same, fs))
-    conclude(jnp.where(outer, fs, same))
-    conclude(far)
+    conclude(jnp.where(outer, fs, far))
+    conclude(jnp.where(outer, far, fs))
+    conclude(same)
 
     for copy in sent:
         copy.wait_send()

time: 150 us -> 146 us (0.973)
  Pallas kernels: 144 us -> 141 us
    pallas_call x1, Pallas kernels: 144 us -> 141 us  [pair_shards(): pl.pallas_call(pair_kernel, out_shape=jax.ShapeDtypeStruct((length, group...]
where the time goes in v3:
time: 146 us
  Pallas kernels  141 us (97%)
  local copies, waits for them, and re-layouts  4.59 us (3%)
    pallas_call x1, Pallas kernels, pair_shards(): pl.pallas_call(pair_kernel, out_shape=jax.ShapeDtypeStruct((length, group...  141 us

profile of v3, /device:TPU:0, one launch (start us, length us, event | category | flops | bytes accessed | tf_op | source)
XLA Modules:
  0.0 145.7 jit_solution(15296560615855344317)
XLA Ops:
  0.0 2.1 %copy.16 = bf16[96,8,4,128]{3,1,2,0:T(8,128)(2,1)} copy(bf16[96,8,4,128]{3,2,1,0:T(4,128)(2,1)} %bitcast.6) | data formatting | bytes 1572864
  2.1 141.1 %shard_map.127 = bf16[768,512]{1,0:T(8,128)(2,1)} custom-call(bf16[768,512]{1,0:T(8,128)(2,1)} %bitcast.5, f32[4,128]{1,0:T(4,128)} %mixer_gain.1, f32[4,128]{1,0:T(4,128)} %pool_scale.1, f32[4,128]{1,0:T(4,128)} %channel_gain.1, f32[4,128]{1,0:T(4,128)} %down_scale.1, f32[1,384]{1,0:T(1,128)} %gate_scale.1, f32[1,384]{1,0:T(1,128)} %up_scale.1, ...), custom_call_target="tpu_custom_call" | custom-call | tf_op jit(solution)/shard_map/pallas_call | solution.py:1113
  143.3 2.4 %reshape.7 = bf16[1,768,4,128]{3,2,1,0:T(4,128)(2,1)} reshape(bf16[768,512]{1,0:T(8,128)(2,1)} %shard_map.127) | data formatting | bytes 1572864 | tf_op jit(solution)/shard_map/reshape | solution.py:1166

commit v4 on v3

--- a/solution.py
+++ b/solution.py
@@ -11,7 +11,7 @@
 EPSILON = 1e-05
 SUBS = 2
 COLUMNS = 256
-VMEM_BYTES = 62 * 1024 * 1024
+VMEM_BYTES = 63 * 1024 * 1024 + 896 * 1024
 F32 = jnp.float32
 BF16 = jnp.bfloat16
 
@@ -469,7 +469,6 @@
 
 
 BAND = 256
-PIECES = 4
 TOKEN_PARTS = 2
 
 
@@ -478,16 +477,19 @@
     mixer_gain,
     pool_scale,
     channel_gain,
-    down_scale,
+    down_scale_own,
     gate_scale,
     up_scale,
-    gate_taps,
-    up_taps,
+    gate_taps_own,
+    up_taps_own,
     pool_own,
     gate_own,
     up_own,
     down_own,
     out,
+    down_scale,
+    gate_taps,
+    up_taps,
     stage_own,
     stage_other,
     stage_down,
@@ -553,8 +555,9 @@
     width = groups * channels
     rows = gate_own.shape[0]
     half_rows = rows // 2
-    half_hidden = gate_own.shape[1] // 2
-    chunks = half_hidden // 128
+    chunks = gate_own.shape[1] // 128
+    few = chunks * 5 // 12
+    many = chunks - few
     half_columns = down_own.shape[1] // 2
     member = lax.rem(fs, 2)
     side = tp // 2
@@ -567,6 +570,11 @@
     sources = (same, far, partner)
     outer = (fs == 0) | (fs == 3)
     inner = jnp.logical_not(outer)
+    count = jnp.where(outer, few, many)
+    other_count = chunks - count
+    begin = jnp.where(outer, many, 0)
+    skip = jnp.where(outer, many - few, 0)
+    other_skip = many - few - skip
 
     sent = []
 
@@ -593,12 +601,18 @@
         copy.start()
         return copy
 
-    mine = aligned(member * half_hidden, half_hidden)
-    theirs = aligned((1 - member) * half_hidden, half_hidden)
+    barrier = pltpu.get_barrier_semaphore()
+    peers = (mirror, sibling, across, diagonal) + tuple({"fs": f} for f in sources)
+    for device in peers:
+        pl.semaphore_signal(
+            barrier, inc=1, device_id=device, device_id_type=pl.DeviceIdType.MESH
+        )
+    mine = pl.ds(pl.multiple_of(jnp.where(outer, few, 0) * 128, 128), many * 128)
+    theirs = pl.ds(pl.multiple_of(jnp.where(outer, 0, few) * 128, 128), many * 128)
     rep_rows = aligned(rep * half_rows, half_rows)
     rep_columns = aligned(rep * half_columns, half_columns)
+    load_pool = local_copy(pool_own, stage_pool, 1)
     load_tokens = local_copy(residual, tokens.at[0, tp], 0)
-    load_pool = local_copy(pool_own, stage_pool, 1)
     loads = [
         local_copy(gate_own.at[:, mine], stage_own.at[0], 2),
         local_copy(up_own.at[:, mine], stage_own.at[1], 3),
@@ -610,17 +624,21 @@
         local_copy(down_own.at[theirs, rep_columns], stage_down_other, 7),
     ]
 
-    barrier = pltpu.get_barrier_semaphore()
-    peers = (mirror, sibling, across, diagonal) + tuple({"fs": f} for f in sources)
-    for device in peers:
-        pl.semaphore_signal(
-            barrier, inc=1, device_id=device, device_id_type=pl.DeviceIdType.MESH
-        )
-    small_all[tp, 0] = mixer_gain[...]
-    small_all[tp, 1] = pool_scale[...]
-    small_all[tp, 2] = channel_gain[...]
-    scales_all[fs, 0] = gate_scale[...]
-    scales_all[fs, 1] = up_scale[...]
+    small_loads = [
+        local_copy(src, dst, 9 + at)
+        for at, (src, dst) in enumerate(
+            (
+                (mixer_gain, small_all.at[tp, 0]),
+                (pool_scale, small_all.at[tp, 1]),
+                (channel_gain, small_all.at[tp, 2]),
+                (gate_scale, scales_all.at[fs, 0]),
+                (up_scale, scales_all.at[fs, 1]),
+                (down_scale_own, down_scale),
+                (gate_taps_own, gate_taps),
+                (up_taps_own, up_taps),
+            )
+        )
+    ]
     load_pool.wait()
     pool_near[...] = stage_pool[...].astype(BF16)
     load_tokens.wait()
@@ -674,18 +692,27 @@
 
     def chunk_copy(j, q):
         target = chunk_target(j, fs, rep)
-        source = target if q == 0 else other.at[j]
+        source = target if q == 1 else other.at[j]
         return remote(source, target, gz_send.at[j, q], gz_recv.at[j, q], {"fs": sources[q]})
 
-    def down_part(shard, half, sub):
-        span = half_hidden // PIECES
-        return down_full.at[shard, half, pl.ds(sub * span, span)]
-
-    def down_copy(q, sub):
-        span = half_hidden // PIECES
-        target = down_part(fs, rep, sub)
-        source = target if q == 0 else down_other.at[pl.ds(sub * span, span)]
-        return remote(source, target, dz_send.at[q, sub], dz_recv.at[q, sub], {"fs": sources[q]})
+    def down_part(shard, half, unit):
+        return down_full.at[shard, half, aligned(unit * 128, 128)]
+
+    def down_copy(q, unit):
+        target = down_part(fs, rep, unit)
+        source = down_other.at[aligned(unit * 128, 128)]
+        return remote(source, target, dz_send.at[q, unit], dz_recv.at[q, unit], {"fs": sources[q]})
+
+    def slice_part(shard, half, unit, lane):
+        return down_full.at[
+            shard, half, aligned(unit * 128, 128), pl.ds(lane * local, local)
+        ]
+
+    def slice_copy(unit, lane):
+        piece = slice_part(fs, rep, unit, lane)
+        return remote(
+            piece, piece, dz_send.at[1 + 2 * lane, unit], dz_recv.at[1 + 2 * lane, unit], {"fs": far}
+        )
 
     def token_copy(part):
         return remote(
@@ -698,38 +725,72 @@
 
     for part in range(TOKEN_PARTS):
         token_copy(part).start()
-    for load in loads:
+    for load in loads + small_loads:
         load.wait()
 
-    @pl.loop(0, chunks)
+    @pl.loop(0, many)
     def _(j):
-        columns = aligned(j * 128, 128)
-        for at in range(2):
-            lanes = slice(at * 128, (at + 1) * 128)
-            weights[j, fs, :, lanes] = stage_own[at, :, columns].astype(BF16)
-            other[j, :, lanes] = stage_other[at, :, columns].astype(BF16)
-        chunk_copy(j, 2).start()
-        pl.when(inner)(chunk_copy(j, 1).start)
+        @pl.when(j < other_count)
+        def _():
+            columns = aligned((other_skip + j) * 128, 128)
+            for at in range(2):
+                lanes = slice(at * 128, (at + 1) * 128)
+                other[j, :, lanes] = stage_other[at, :, columns].astype(BF16)
+            chunk_copy(j, 2).start()
+
+        @pl.when(j < count)
+        def _():
+            columns = aligned((skip + j) * 128, 128)
+            for at in range(2):
+                lanes = slice(at * 128, (at + 1) * 128)
+                weights[j, fs, :, lanes] = stage_own[at, :, columns].astype(BF16)
+            pl.when(inner)(chunk_copy(j, 1).start)
 
     @pl.when(inner)
     def _():
-        @pl.loop(0, chunks)
+        @pl.loop(0, other_count)
         def _(j):
             chunk_copy(j, 0).start()
 
     for load in load_down:
         load.wait()
-    for half in range(2):
-        down_full[fs, half] = stage_down[
-            :, half * half_columns : (half + 1) * half_columns
-        ].astype(BF16)
-    down_other[...] = stage_down_other[...].astype(BF16)
+    hidden[:, few * 128 :] = jnp.zeros((2 * length, (many - few) * 128), BF16)
+
+    @pl.when(outer)
+    def _():
+        down_full[:, :, few * 128 :] = jnp.zeros(
+            (4, 2, (many - few) * 128, half_columns), BF16
+        )
+
+    @pl.loop(0, count)
+    def _(j):
+        here = aligned(j * 128, 128)
+        there = aligned((skip + j) * 128, 128)
+        for half in range(2):
+            down_full[fs, half, here] = stage_down[
+                there, half * half_columns : (half + 1) * half_columns
+            ].astype(BF16)
+
+    @pl.loop(0, other_count)
+    def _(j):
+        there = aligned((other_skip + j) * 128, 128)
+        down_other[aligned(j * 128, 128)] = stage_down_other[there].astype(BF16)
 
     @pl.when(inner)
     def _():
-        for q in (2, 0, 1):
-            for sub in range(PIECES):
-                down_copy(q, sub).start()
+        @pl.loop(0, other_count)
+        def _(unit):
+            down_copy(2, unit).start()
+
+        @pl.loop(0, other_count)
+        def _(unit):
+            down_copy(0, unit).start()
+
+        for lane in range(2):
+
+            @pl.loop(0, count)
+            def _(unit):
+                slice_copy(unit, lane).start()
 
     def landed(ref, send, recv):
         remote(ref, ref, send, recv, mirror).wait_recv()
@@ -743,14 +804,27 @@
         landed(piece, gz_send.at[j, q], gz_recv.at[j, q])
         chunk_onward(j, q, shard).start()
 
-    def down_onward(q, shard, sub):
-        piece = down_part(shard, rep, sub)
-        return remote(piece, piece, dx_send.at[q, sub], dx_recv.at[q, sub], mirror)
-
-    def forward_down(q, shard, subs=range(PIECES)):
-        for sub in subs:
-            landed(down_part(shard, rep, sub), dz_send.at[q, sub], dz_recv.at[q, sub])
-            down_onward(q, shard, sub).start()
+    def down_onward(q, shard, unit):
+        piece = down_part(shard, rep, unit)
+        return remote(piece, piece, dx_send.at[q, unit], dx_recv.at[q, unit], mirror)
+
+    def slice_onward(unit, lane):
+        piece = slice_part(far, rep, unit, lane)
+        sem = (1 + 2 * lane, unit)
+        return remote(piece, piece, dx_send.at[sem], dx_recv.at[sem], mirror)
+
+    def forward_slice(lane, low=0, high=many):
+        @pl.loop(low, jnp.minimum(count, high))
+        def _(unit):
+            sem = (1 + 2 * lane, unit)
+            landed(slice_part(far, rep, unit, lane), dz_send.at[sem], dz_recv.at[sem])
+            slice_onward(unit, lane).start()
+
+    def forward_down(q, shard, low=0, high=many):
+        @pl.loop(low, jnp.minimum(count, high))
+        def _(unit):
+            landed(down_part(shard, rep, unit), dz_send.at[q, unit], dz_recv.at[q, unit])
+            down_onward(q, shard, unit).start()
 
     for q, f in ((2, partner), (1, far), (0, same)):
         piece = pool_part(f, rep)
@@ -784,20 +858,20 @@
         for j in range(low, high):
             forward_chunk(j, kind, shard)
 
-    third = chunks // 3
+    third = many // 3
     own_onward(0)
     pl.when(inner)(functools.partial(forward_chunks, 1, far, 0, third))
     partner_onward(0)
     own_onward(1)
-    pl.when(inner)(functools.partial(forward_chunks, 1, far, third, chunks - 1))
+    pl.when(inner)(functools.partial(forward_chunks, 1, far, third, many - third))
     partner_onward(1)
-    pl.when(inner)(functools.partial(forward_chunks, 1, far, chunks - 1, chunks))
+    pl.when(inner)(functools.partial(forward_chunks, 1, far, many - third, many))
     second_kind, second = jnp.where(outer, 0, 2), jnp.where(outer, same, partner)
-    forward_chunks(second_kind, second, 0, 2)
+    forward_chunks(second_kind, second, 0, few - 3)
     slab = pool_slab(t_across)
     landed(slab, pt_send.at[1], pt_recv.at[1])
     start(slab, slab, pt_send.at[2], pt_recv.at[2], sibling)
-    forward_chunks(second_kind, second, 2, chunks // 2)
+    forward_chunks(second_kind, second, few - 3, few - 2)
 
     for part in range(TOKEN_PARTS):
         landed(token_part(0, t_sibling, part), rs_send.at[0, part], rs_recv.at[0, part])
@@ -868,19 +942,22 @@
                     inputs[span, columns].astype(F32) * factor * small_all[t, 2, g : g + 1]
                 ).astype(BF16)
 
-    mix(0, functools.partial(forward_chunks, second_kind, second, chunks // 2, chunks // 2 + 1))
-    forward_chunks(second_kind, second, chunks // 2 + 1, chunks)
-
-    @pl.when(outer)
-    def _():
-        @pl.loop(0, chunks)
-        def _(j):
-            chunk_copy(j, 1).start()
-            chunk_copy(j, 0).start()
-
-        for sub in range(PIECES):
-            down_copy(2, sub).start()
-
+    def cross():
+        forward_chunks(second_kind, second, few - 2, few)
+
+        @pl.when(outer)
+        def _():
+            @pl.loop(0, many)
+            def _(j):
+                pl.when(j < few)(chunk_copy(j, 1).start)
+                chunk_copy(j, 0).start()
+
+            @pl.loop(0, many)
+            def _(unit):
+                down_copy(2, unit).start()
+
+    mix(0, cross)
+    pl.when(inner)(functools.partial(forward_chunks, 2, partner, few, many))
     for part in range(TOKEN_PARTS):
         piece = token_part(1, t_across, part)
         landed(piece, ry_send.at[1, part], ry_recv.at[1, part])
@@ -905,8 +982,8 @@
     def expand(j):
         for q, f in enumerate(sources):
             landed(chunk_target(j, f, 1 - rep), gx_send.at[j, q], gx_recv.at[j, q])
-        here = aligned(member * half_hidden + j * 128, 128)
-        unit = member * chunks + j
+        unit = begin + j
+        here = aligned(unit * 128, 128)
         scale_at = aligned(lax.rem(unit, thirds) * 128, 128)
         taps = [
             table[:, here] * scales_all[unit // thirds, at, :, scale_at]
@@ -921,20 +998,26 @@
             silu = conv_gate / (1.0 + jnp.exp(-conv_gate))
             hidden[span, aligned(j * 128, 128)] = (silu * conv_up).astype(BF16)
 
-    @pl.loop(0, chunks)
+    @pl.loop(0, count)
     def _(j):
         expand(j)
 
-        @pl.when(j < chunks - 2)
+        @pl.when(j < count - 2)
         def _():
             forward_late(j + 2)
 
-        @pl.when(outer & (j == chunks - 2))
+        @pl.when(outer & (j == few - 2))
         def _():
             forward_down(0, same)
-            for sub in range(PIECES):
-                down_copy(1, sub).start()
-                down_copy(0, sub).start()
+
+            @pl.loop(0, many)
+            def _(unit):
+                @pl.when(unit < few)
+                def _():
+                    for lane in range(2):
+                        slice_copy(unit, lane).start()
+
+                down_copy(0, unit).start()
 
     def core_copy(shard, half, slot):
         return remote(
@@ -954,6 +1037,24 @@
             give[shard, half, slot] = jnp.where(core == 0, high, low).astype(BF16)
             core_copy(shard, half, slot).start()
 
+    def far_product(half, lane):
+        for slot in (1, 0):
+            span = slice(slot * length, (slot + 1) * length)
+            made = jnp.dot(
+                hidden[span],
+                down_full[far, half, :, lane * local : (lane + 1) * local],
+                preferred_element_type=F32,
+            )
+
+            @pl.when(core == lane)
+            def _():
+                keep[far, half, slot] = made
+
+            @pl.when(core != lane)
+            def _():
+                give[far, half, slot] = made.astype(BF16)
+                core_copy(far, half, slot).start()
+
     def y_copy(shard, slot):
         return remote(
             y_out.at[shard, slot],
@@ -964,8 +1065,9 @@
         )
 
     def arrived_x(q, shard):
-        for sub in range(PIECES):
-            landed(down_part(shard, 1 - rep, sub), dx_send.at[q, sub], dx_recv.at[q, sub])
+        @pl.loop(0, count)
+        def _(unit):
+            landed(down_part(shard, 1 - rep, unit), dx_send.at[q, unit], dx_recv.at[q, unit])
 
     def join_cores(shard, half):
         for slot in (1, 0):
@@ -1006,38 +1108,59 @@
     early, early_kind = jnp.where(outer, same, partner), jnp.where(outer, 0, 2)
     later, later_kind = jnp.where(outer, partner, same), jnp.where(outer, 2, 0)
 
-    def pass_on(sub):
-        pl.when(outer)(functools.partial(forward_down, 2, partner, (sub,)))
-        forward_down(late_kind, late, (sub,))
-
+    def pass_on(step):
+        low, high = 2 * step, min(2 * step + 2, many)
+
+        @pl.when(outer)
+        def _():
+            forward_down(2, partner, low, high)
+            for lane in range(2):
+                forward_slice(lane, low, high)
+
+        pl.when(inner)(functools.partial(forward_down, 0, same, low, high))
+
+    pl.when(inner)(functools.partial(forward_down, 2, partner))
     product(fs, rep)
     product(fs, 1 - rep)
     join_cores(fs, rep)
-    pl.when(inner)(functools.partial(forward_down, 2, partner))
+    pass_on(0)
     join_cores(fs, 1 - rep)
     product(early, rep)
-    pass_on(0)
+    pass_on(1)
     arrived_x(early_kind, early)
     product(early, 1 - rep)
     join_cores(early, rep)
-    pass_on(1)
+    pass_on(2)
     join_cores(early, 1 - rep)
-    pass_on(2)
+    pass_on(3)
     join_sides(fs)
-    pass_on(3)
     product(later, rep)
-    pl.when(inner)(functools.partial(forward_down, 1, far, (0, 1)))
+    pl.when(inner)(functools.partial(forward_slice, 0))
     arrived_x(later_kind, later)
     product(later, 1 - rep)
+    pl.when(inner)(functools.partial(forward_slice, 1, 0, many // 2))
     join_cores(later, rep)
-    pl.when(inner)(functools.partial(forward_down, 1, far, (2, 3)))
     join_cores(later, 1 - rep)
-    join_sides(early)
-    product(far, rep)
-    arrived_x(1, far)
-    product(far, 1 - rep)
-    join_cores(far, rep)
-    join_cores(far, 1 - rep)
+    far_product(rep, 0)
+    pl.when(inner)(functools.partial(forward_slice, 1, many // 2, many))
+    for lane in range(2):
+        if lane:
+            far_product(rep, lane)
+
+        @pl.loop(0, count)
+        def _(unit):
+            sem = (1 + 2 * lane, unit)
+            landed(slice_part(far, 1 - rep, unit, lane), dx_send.at[sem], dx_recv.at[sem])
+
+        far_product(1 - rep, lane)
+
+        @pl.when(core == lane)
+        def _():
+            join_cores(far, rep)
+            join_cores(far, 1 - rep)
+
+        if lane == 0:
+            join_sides(early)
     join_sides(later)
     join_sides(far)
     conclude(partner)
@@ -1056,16 +1179,28 @@
             y_copy(shard, slot).wait_send()
             for half in range(2):
                 core_copy(shard, half, slot).wait_send()
-    for q, f in enumerate(sources):
-        for sub in range(PIECES):
-            down_copy(q, sub).wait_send()
-            down_onward(q, f, sub).wait_send()
-
-    @pl.loop(0, chunks)
+
+    @pl.loop(0, many)
     def _(j):
         for q, f in enumerate(sources):
-            chunk_copy(j, q).wait_send()
-            chunk_onward(j, q, f).wait_send()
+
+            @pl.when(j < (count if q == 1 else other_count))
+            def _():
+                chunk_copy(j, q).wait_send()
+                if q == 1:
+                    for lane in range(2):
+                        slice_copy(j, lane).wait_send()
+                else:
+                    down_copy(q, j).wait_send()
+
+            @pl.when(j < count)
+            def _():
+                chunk_onward(j, q, f).wait_send()
+                if q == 1:
+                    for lane in range(2):
+                        slice_onward(j, lane).wait_send()
+                else:
+                    down_onward(q, f, j).wait_send()
 
 
 def pair_shards(
@@ -1087,8 +1222,9 @@
     channels = local * 4
     width = groups * channels
     rows, hidden_width = gate_weight.shape
-    half = hidden_width // 2
-    chunks = half // 128
+    chunks = hidden_width // 128
+    chunks = chunks - chunks * 5 // 12
+    half = chunks * 128
     half_columns = down_weight.shape[1] // 2
     vmem = pl.BlockSpec(memory_space=pltpu.VMEM)
     anywhere = pl.BlockSpec(memory_space=pl.ANY)
@@ -1104,8 +1240,8 @@
         (4, TOKEN_PARTS),
         (chunks, 3),
         (chunks, 3),
-        (3, PIECES),
-        (3, PIECES),
+        (4, chunks),
+        (4, chunks),
         (4, 2, 2),
         (4, 2),
         (4,),
@@ -1113,9 +1249,12 @@
     out = pl.pallas_call(
         pair_kernel,
         out_shape=jax.ShapeDtypeStruct((length, groups * local), BF16),
-        in_specs=[anywhere] + [vmem] * 8 + [anywhere] * 4,
+        in_specs=[anywhere] * 13,
         out_specs=vmem,
         scratch_shapes=[
+            pltpu.VMEM(down_scale.shape, F32),
+            pltpu.VMEM(gate_taps.shape, F32),
+            pltpu.VMEM(up_taps.shape, F32),
             pltpu.VMEM((2, rows, half), F32),
             pltpu.VMEM((2, rows // 2, half), F32),
             pltpu.VMEM((half, 2 * half_columns), F32),
@@ -1144,7 +1283,7 @@
             pltpu.VMEM((4, length, local), BF16),
         ]
         + [dma(shape) for shape in pairs for _ in range(2)]
-        + [dma((9,))],
+        + [dma((17,))],
         compiler_params=pltpu.CompilerParams(
             collective_id=0, has_side_effects=True, vmem_limit_bytes=VMEM_BYTES
         ),
@@ -1176,7 +1315,7 @@
         and groups == len(WINDOWS)
         and down_weight[1] == 4 * local
         and gate_weight[0] * 4 == groups * local * 4
-        and gate_weight[1] % 512 == 0
+        and gate_weight[1] % 1536 == 0
     )
 
 

time: 146 us -> 145 us (level); the launches traced: 146 us -> 143 us
  Pallas kernels: 141 us -> 138 us
    pallas_call x1, Pallas kernels: 141 us -> 138 us  [pair_shards(): pl.pallas_call(pair_kernel, out_shape=jax.ShapeDtypeStruct((length, group...]
where the time goes in v4:
time: 145 us; the launch traced here: 143 us
  Pallas kernels  138 us (95%)
  local copies, waits for them, and re-layouts  4.59 us (3%)
    pallas_call x1, Pallas kernels, pair_shards(): pl.pallas_call(pair_kernel, out_shape=jax.ShapeDtypeStruct((length, group...  138 us

profile of v4, /device:TPU:0, one launch (start us, length us, event | category | flops | bytes accessed | tf_op | source)
XLA Modules:
  0.0 142.8 jit_solution(11114227963023429715)
XLA Ops:
  0.0 2.1 %copy.16 = bf16[96,8,4,128]{3,1,2,0:T(8,128)(2,1)} copy(bf16[96,8,4,128]{3,2,1,0:T(4,128)(2,1)} %bitcast.6) | data formatting | bytes 1572864
  2.1 138.2 %shard_map.127 = bf16[768,512]{1,0:T(8,128)(2,1)} custom-call(bf16[768,512]{1,0:T(8,128)(2,1)} %bitcast.5, f32[4,128]{1,0:T(4,128)} %mixer_gain.1, f32[4,128]{1,0:T(4,128)} %pool_scale.1, f32[4,128]{1,0:T(4,128)} %channel_gain.1, f32[4,128]{1,0:T(4,128)} %down_scale_own.1, f32[1,384]{1,0:T(1,128)} %gate_scale.1, f32[1,384]{1,0:T(1,128)} %up_scale.1, ...), custom_call_target="tpu_custom_call" | custom-call | tf_op jit(solution)/shard_map/pallas_call | solution.py:1249
  140.4 2.4 %reshape.7 = bf16[1,768,4,128]{3,2,1,0:T(4,128)(2,1)} reshape(bf16[768,512]{1,0:T(8,128)(2,1)} %shard_map.127) | data formatting | bytes 1572864 | tf_op jit(solution)/shard_map/reshape | solution.py:1305

commit v5 on v4

--- a/solution.py
+++ b/solution.py
@@ -469,6 +469,7 @@
 
 
 BAND = 256
+FEW = 5
 TOKEN_PARTS = 2
 
 
@@ -556,7 +557,7 @@
     rows = gate_own.shape[0]
     half_rows = rows // 2
     chunks = gate_own.shape[1] // 128
-    few = chunks * 5 // 12
+    few = chunks * FEW // 12
     many = chunks - few
     half_columns = down_own.shape[1] // 2
     member = lax.rem(fs, 2)
@@ -754,13 +755,14 @@
 
     for load in load_down:
         load.wait()
-    hidden[:, few * 128 :] = jnp.zeros((2 * length, (many - few) * 128), BF16)
-
-    @pl.when(outer)
-    def _():
-        down_full[:, :, few * 128 :] = jnp.zeros(
-            (4, 2, (many - few) * 128, half_columns), BF16
-        )
+    if many > few:
+        hidden[:, few * 128 :] = jnp.zeros((2 * length, (many - few) * 128), BF16)
+
+        @pl.when(outer)
+        def _():
+            down_full[:, :, few * 128 :] = jnp.zeros(
+                (4, 2, (many - few) * 128, half_columns), BF16
+            )
 
     @pl.loop(0, count)
     def _(j):
@@ -775,6 +777,11 @@
     def _(j):
         there = aligned((other_skip + j) * 128, 128)
         down_other[aligned(j * 128, 128)] = stage_down_other[there].astype(BF16)
+
+    @pl.when(outer)
+    def _():
+        for unit in range(2):
+            down_copy(2, unit).start()
 
     @pl.when(inner)
     def _():
@@ -952,12 +959,17 @@
                 pl.when(j < few)(chunk_copy(j, 1).start)
                 chunk_copy(j, 0).start()
 
-            @pl.loop(0, many)
+            @pl.loop(2, many)
             def _(unit):
                 down_copy(2, unit).start()
 
     mix(0, cross)
-    pl.when(inner)(functools.partial(forward_chunks, 2, partner, few, many))
+
+    @pl.when(inner)
+    def _():
+        forward_chunks(2, partner, few, many)
+        forward_down(2, partner, 0, 2)
+
     for part in range(TOKEN_PARTS):
         piece = token_part(1, t_across, part)
         landed(piece, ry_send.at[1, part], ry_recv.at[1, part])
@@ -1006,18 +1018,27 @@
         def _():
             forward_late(j + 2)
 
+        @pl.when(inner & (j == many - 3))
+        def _():
+            forward_down(2, partner, 2, 4)
+
+        @pl.when(inner & (j == many - 2))
+        def _():
+            forward_down(2, partner, 4, 6)
+
         @pl.when(outer & (j == few - 2))
         def _():
             forward_down(0, same)
 
             @pl.loop(0, many)
             def _(unit):
-                @pl.when(unit < few)
-                def _():
-                    for lane in range(2):
-                        slice_copy(unit, lane).start()
-
                 down_copy(0, unit).start()
+
+            for lane in range(2):
+
+                @pl.loop(0, few)
+                def _(unit):
+                    slice_copy(unit, lane).start()
 
     def core_copy(shard, half, slot):
         return remote(
@@ -1029,6 +1050,16 @@
         )
 
     def product(shard, half):
+        made = jnp.dot(hidden[...], down_full[shard, half], preferred_element_type=F32)
+        for slot in (1, 0):
+            span = slice(slot * length, (slot + 1) * length)
+            low, high = made[span, :local], made[span, local:]
+            keep[shard, half, slot] = jnp.where(core == 0, low, high)
+            give[shard, half, slot] = jnp.where(core == 0, high, low).astype(BF16)
+        for slot in (1, 0):
+            core_copy(shard, half, slot).start()
+
+    def product_by_slot(shard, half):
         for slot in (1, 0):
             span = slice(slot * length, (slot + 1) * length)
             made = jnp.dot(hidden[span], down_full[shard, half], preferred_element_type=F32)
@@ -1037,31 +1068,28 @@
             give[shard, half, slot] = jnp.where(core == 0, high, low).astype(BF16)
             core_copy(shard, half, slot).start()
 
-    def far_product(half, lane):
-        for slot in (1, 0):
-            span = slice(slot * length, (slot + 1) * length)
-            made = jnp.dot(
-                hidden[span],
-                down_full[far, half, :, lane * local : (lane + 1) * local],
-                preferred_element_type=F32,
-            )
-
-            @pl.when(core == lane)
-            def _():
-                keep[far, half, slot] = made
-
-            @pl.when(core != lane)
-            def _():
-                give[far, half, slot] = made.astype(BF16)
-                core_copy(far, half, slot).start()
-
-    def y_copy(shard, slot):
+    def y_part(buffer, shard, which):
+        if which == 0:
+            return buffer.at[shard, 0]
+        return buffer.at[shard, 1, pl.ds((which - 1) * (length // 2), length // 2)]
+
+    def y_copy(shard, which):
         return remote(
-            y_out.at[shard, slot],
-            y_in.at[shard, slot],
-            y_send.at[shard, slot],
-            y_recv.at[shard, slot],
+            y_part(y_out, shard, which),
+            y_part(y_in, shard, which),
+            y_send.at[shard, which],
+            y_recv.at[shard, which],
             across,
+        )
+
+    def z_copy(shard, part):
+        rows = pl.ds(part * (length // 2), length // 2)
+        return remote(
+            z_out.at[shard, rows],
+            z_in.at[shard, rows],
+            z_send.at[shard, part],
+            z_recv.at[shard, part],
+            {"fs": partner},
         )
 
     def arrived_x(q, shard):
@@ -1081,24 +1109,22 @@
             @pl.when(half != side)
             def _():
                 y_out[shard, slot] = total.astype(BF16)
-                y_copy(shard, slot).start()
+                for which in (1, 2) if slot else (0,):
+                    y_copy(shard, which).start()
 
     def join_sides(shard):
-        y_copy(shard, 1).wait_recv()
-        total = keep[shard, side, 1] + y_in[shard, 1].astype(F32)
-        z_out[shard] = total.astype(BF16)
-        start(
-            z_out.at[shard],
-            z_in.at[shard],
-            z_send.at[shard],
-            z_recv.at[shard],
-            {"fs": partner},
-        )
+        for part in range(2):
+            rows = slice(part * (length // 2), (part + 1) * (length // 2))
+            y_copy(shard, 1 + part).wait_recv()
+            total = keep[shard, side, 1, rows] + y_in[shard, 1, rows].astype(F32)
+            z_out[shard, rows] = total.astype(BF16)
+            z_copy(shard, part).start()
 
     def conclude(shard):
         y_copy(shard, 0).wait_recv()
         total = keep[shard, side, 0] + y_in[shard, 0].astype(F32)
-        landed(z_in.at[shard], z_send.at[shard], z_recv.at[shard])
+        for part in range(2):
+            z_copy(shard, part).wait_recv()
         columns = aligned(shard * local, local)
         total = total + z_in[shard].astype(F32)
         out[:, columns] = (
@@ -1110,57 +1136,46 @@
 
     def pass_on(step):
         low, high = 2 * step, min(2 * step + 2, many)
-
-        @pl.when(outer)
-        def _():
-            forward_down(2, partner, low, high)
-            for lane in range(2):
-                forward_slice(lane, low, high)
-
-        pl.when(inner)(functools.partial(forward_down, 0, same, low, high))
-
-    pl.when(inner)(functools.partial(forward_down, 2, partner))
+        forward_down(later_kind, later, low, high)
+
+    pl.when(inner)(functools.partial(forward_down, 2, partner, 6, many))
     product(fs, rep)
     product(fs, 1 - rep)
+    pl.when(inner)(functools.partial(pass_on, 0))
     join_cores(fs, rep)
-    pass_on(0)
     join_cores(fs, 1 - rep)
+    pl.when(outer)(functools.partial(pass_on, 0))
     product(early, rep)
     pass_on(1)
     arrived_x(early_kind, early)
     product(early, 1 - rep)
+    pass_on(2)
+    pl.when(inner)(functools.partial(pass_on, 3))
     join_cores(early, rep)
-    pass_on(2)
     join_cores(early, 1 - rep)
-    pass_on(3)
+    pl.when(inner)(functools.partial(forward_slice, 0, 0, 3))
+    product(later, rep)
     join_sides(fs)
-    product(later, rep)
-    pl.when(inner)(functools.partial(forward_slice, 0))
+    pl.when(outer)(functools.partial(forward_slice, 0, 0, 3))
+    forward_slice(0, 3)
     arrived_x(later_kind, later)
     product(later, 1 - rep)
-    pl.when(inner)(functools.partial(forward_slice, 1, 0, many // 2))
     join_cores(later, rep)
+    forward_slice(1, 0, many // 2)
     join_cores(later, 1 - rep)
-    far_product(rep, 0)
-    pl.when(inner)(functools.partial(forward_slice, 1, many // 2, many))
+    forward_slice(1, many // 2)
+    product(far, rep)
+    join_sides(early)
     for lane in range(2):
-        if lane:
-            far_product(rep, lane)
 
         @pl.loop(0, count)
         def _(unit):
             sem = (1 + 2 * lane, unit)
             landed(slice_part(far, 1 - rep, unit, lane), dx_send.at[sem], dx_recv.at[sem])
 
-        far_product(1 - rep, lane)
-
-        @pl.when(core == lane)
-        def _():
-            join_cores(far, rep)
-            join_cores(far, 1 - rep)
-
-        if lane == 0:
-            join_sides(early)
+    product_by_slot(far, 1 - rep)
+    join_cores(far, rep)
+    join_cores(far, 1 - rep)
     join_sides(later)
     join_sides(far)
     conclude(partner)
@@ -1175,8 +1190,10 @@
     for part in range(TOKEN_PARTS):
         token_copy(part).wait_send()
     for shard in range(4):
+        for which in range(3):
+            y_copy(shard, which).wait_send()
         for slot in range(2):
-            y_copy(shard, slot).wait_send()
+            z_copy(shard, slot).wait_send()
             for half in range(2):
                 core_copy(shard, half, slot).wait_send()
 
@@ -1223,7 +1240,7 @@
     width = groups * channels
     rows, hidden_width = gate_weight.shape
     chunks = hidden_width // 128
-    chunks = chunks - chunks * 5 // 12
+    chunks = chunks - chunks * FEW // 12
     half = chunks * 128
     half_columns = down_weight.shape[1] // 2
     vmem = pl.BlockSpec(memory_space=pltpu.VMEM)
@@ -1243,8 +1260,8 @@
         (4, chunks),
         (4, chunks),
         (4, 2, 2),
+        (4, 3),
         (4, 2),
-        (4,),
     ]
     out = pl.pallas_call(
         pair_kernel,

time: 145 us -> 143 us (0.986); the launches traced: 143 us -> 143 us
  no operation moved by 1% of the time
where the time goes in v5:
time: 143 us
  Pallas kernels  138 us (97%)
  local copies, waits for them, and re-layouts  4.59 us (3%)
    pallas_call x1, Pallas kernels, pair_shards(): pl.pallas_call(pair_kernel, out_shape=jax.ShapeDtypeStruct((length, group...  138 us

profile of v5, /device:TPU:0, one launch (start us, length us, event | category | flops | bytes accessed | tf_op | source)
XLA Modules:
  0.0 142.8 jit_solution(15908745966327290608)
XLA Ops:
  0.0 2.1 %copy.16 = bf16[96,8,4,128]{3,1,2,0:T(8,128)(2,1)} copy(bf16[96,8,4,128]{3,2,1,0:T(4,128)(2,1)} %bitcast.6) | data formatting | bytes 1572864
  2.1 138.2 %shard_map.127 = bf16[768,512]{1,0:T(8,128)(2,1)} custom-call(bf16[768,512]{1,0:T(8,128)(2,1)} %bitcast.5, f32[4,128]{1,0:T(4,128)} %mixer_gain.1, f32[4,128]{1,0:T(4,128)} %pool_scale.1, f32[4,128]{1,0:T(4,128)} %channel_gain.1, f32[4,128]{1,0:T(4,128)} %down_scale_own.1, f32[1,384]{1,0:T(1,128)} %gate_scale.1, f32[1,384]{1,0:T(1,128)} %up_scale.1, ...), custom_call_target="tpu_custom_call" | custom-call | tf_op jit(solution)/shard_map/pallas_call | solution.py:1266
  140.3 2.4 %reshape.7 = bf16[1,768,4,128]{3,2,1,0:T(4,128)(2,1)} reshape(bf16[768,512]{1,0:T(8,128)(2,1)} %shard_map.127) | data formatting | bytes 1572864 | tf_op jit(solution)/shard_map/reshape | solution.py:1322

commit v6 on v5

--- a/solution.py
+++ b/solution.py
@@ -694,7 +694,7 @@
     def chunk_copy(j, q):
         target = chunk_target(j, fs, rep)
         source = target if q == 1 else other.at[j]
-        return remote(source, target, gz_send.at[j, q], gz_recv.at[j, q], {"fs": sources[q]})
+        return remote(source, target, gz_send.at[0], gz_recv.at[j, q], {"fs": sources[q]})
 
     def down_part(shard, half, unit):
         return down_full.at[shard, half, aligned(unit * 128, 128)]
@@ -702,7 +702,7 @@
     def down_copy(q, unit):
         target = down_part(fs, rep, unit)
         source = down_other.at[aligned(unit * 128, 128)]
-        return remote(source, target, dz_send.at[q, unit], dz_recv.at[q, unit], {"fs": sources[q]})
+        return remote(source, target, dz_send.at[0], dz_recv.at[q, unit], {"fs": sources[q]})
 
     def slice_part(shard, half, unit, lane):
         return down_full.at[
@@ -712,7 +712,7 @@
     def slice_copy(unit, lane):
         piece = slice_part(fs, rep, unit, lane)
         return remote(
-            piece, piece, dz_send.at[1 + 2 * lane, unit], dz_recv.at[1 + 2 * lane, unit], {"fs": far}
+            piece, piece, dz_send.at[0], dz_recv.at[1 + 2 * lane, unit], {"fs": far}
         )
 
     def token_copy(part):
@@ -804,33 +804,33 @@
 
     def chunk_onward(j, q, shard):
         piece = chunk_target(j, shard, rep)
-        return remote(piece, piece, gx_send.at[j, q], gx_recv.at[j, q], mirror)
+        return remote(piece, piece, gx_send.at[0], gx_recv.at[j, q], mirror)
 
     def forward_chunk(j, q, shard):
         piece = chunk_target(j, shard, rep)
-        landed(piece, gz_send.at[j, q], gz_recv.at[j, q])
+        landed(piece, gz_send.at[0], gz_recv.at[j, q])
         chunk_onward(j, q, shard).start()
 
     def down_onward(q, shard, unit):
         piece = down_part(shard, rep, unit)
-        return remote(piece, piece, dx_send.at[q, unit], dx_recv.at[q, unit], mirror)
+        return remote(piece, piece, dx_send.at[0], dx_recv.at[q, unit], mirror)
 
     def slice_onward(unit, lane):
         piece = slice_part(far, rep, unit, lane)
         sem = (1 + 2 * lane, unit)
-        return remote(piece, piece, dx_send.at[sem], dx_recv.at[sem], mirror)
+        return remote(piece, piece, dx_send.at[0], dx_recv.at[sem], mirror)
 
     def forward_slice(lane, low=0, high=many):
         @pl.loop(low, jnp.minimum(count, high))
         def _(unit):
             sem = (1 + 2 * lane, unit)
-            landed(slice_part(far, rep, unit, lane), dz_send.at[sem], dz_recv.at[sem])
+            landed(slice_part(far, rep, unit, lane), dz_send.at[0], dz_recv.at[sem])
             slice_onward(unit, lane).start()
 
     def forward_down(q, shard, low=0, high=many):
         @pl.loop(low, jnp.minimum(count, high))
         def _(unit):
-            landed(down_part(shard, rep, unit), dz_send.at[q, unit], dz_recv.at[q, unit])
+            landed(down_part(shard, rep, unit), dz_send.at[0], dz_recv.at[q, unit])
             down_onward(q, shard, unit).start()
 
     for q, f in ((2, partner), (1, far), (0, same)):
@@ -993,7 +993,7 @@
 
     def expand(j):
         for q, f in enumerate(sources):
-            landed(chunk_target(j, f, 1 - rep), gx_send.at[j, q], gx_recv.at[j, q])
+            landed(chunk_target(j, f, 1 - rep), gx_send.at[0], gx_recv.at[j, q])
         unit = begin + j
         here = aligned(unit * 128, 128)
         scale_at = aligned(lax.rem(unit, thirds) * 128, 128)
@@ -1044,7 +1044,7 @@
         return remote(
             give.at[shard, half, slot],
             got.at[shard, half, slot],
-            core_send.at[shard, half, slot],
+            core_send.at[0],
             core_recv.at[shard, half, slot],
             sibling,
         )
@@ -1077,7 +1077,7 @@
         return remote(
             y_part(y_out, shard, which),
             y_part(y_in, shard, which),
-            y_send.at[shard, which],
+            y_send.at[0],
             y_recv.at[shard, which],
             across,
         )
@@ -1087,7 +1087,7 @@
         return remote(
             z_out.at[shard, rows],
             z_in.at[shard, rows],
-            z_send.at[shard, part],
+            z_send.at[0],
             z_recv.at[shard, part],
             {"fs": partner},
         )
@@ -1095,7 +1095,7 @@
     def arrived_x(q, shard):
         @pl.loop(0, count)
         def _(unit):
-            landed(down_part(shard, 1 - rep, unit), dx_send.at[q, unit], dx_recv.at[q, unit])
+            landed(down_part(shard, 1 - rep, unit), dx_send.at[0], dx_recv.at[q, unit])
 
     def join_cores(shard, half):
         for slot in (1, 0):
@@ -1171,7 +1171,7 @@
         @pl.loop(0, count)
         def _(unit):
             sem = (1 + 2 * lane, unit)
-            landed(slice_part(far, 1 - rep, unit, lane), dx_send.at[sem], dx_recv.at[sem])
+            landed(slice_part(far, 1 - rep, unit, lane), dx_send.at[0], dx_recv.at[sem])
 
     product_by_slot(far, 1 - rep)
     join_cores(far, rep)
@@ -1189,35 +1189,22 @@
         pool_copy_to(q).wait_send()
     for part in range(TOKEN_PARTS):
         token_copy(part).wait_send()
-    for shard in range(4):
-        for which in range(3):
-            y_copy(shard, which).wait_send()
-        for slot in range(2):
-            z_copy(shard, slot).wait_send()
-            for half in range(2):
-                core_copy(shard, half, slot).wait_send()
-
-    @pl.loop(0, many)
-    def _(j):
-        for q, f in enumerate(sources):
-
-            @pl.when(j < (count if q == 1 else other_count))
-            def _():
-                chunk_copy(j, q).wait_send()
-                if q == 1:
-                    for lane in range(2):
-                        slice_copy(j, lane).wait_send()
-                else:
-                    down_copy(q, j).wait_send()
-
-            @pl.when(j < count)
-            def _():
-                chunk_onward(j, q, f).wait_send()
-                if q == 1:
-                    for lane in range(2):
-                        slice_onward(j, lane).wait_send()
-                else:
-                    down_onward(q, f, j).wait_send()
+    def drained(ref, send, recv):
+        remote(ref, ref, send.at[0], recv, mirror).wait_send()
+
+    drained(y_out, y_send, y_recv.at[0, 0])
+    drained(z_out, z_send, z_recv.at[0, 0])
+    drained(give, core_send, core_recv.at[0, 0, 0])
+
+    def drain(own, others):
+        total = own + 2 * others
+        drained(weights.at[:4, :, pl.ds(0, total * 16)], gz_send, gz_recv.at[0, 0])
+        drained(weights.at[:4, :, pl.ds(0, own * 48)], gx_send, gx_recv.at[0, 0])
+        drained(down_full.at[:2, :, pl.ds(0, total * 32)], dz_send, dz_recv.at[0, 0])
+        drained(down_full.at[:3, 0, pl.ds(0, own * 128)], dx_send, dx_recv.at[0, 0])
+
+    pl.when(inner)(functools.partial(drain, many, few))
+    pl.when(outer)(functools.partial(drain, few, many))
 
 
 def pair_shards(
@@ -1246,7 +1233,7 @@
     vmem = pl.BlockSpec(memory_space=pltpu.VMEM)
     anywhere = pl.BlockSpec(memory_space=pl.ANY)
     dma = pltpu.SemaphoreType.DMA
-    pairs = [
+    shapes = [
         (3, 3),
         (2, 3),
         (3,),
@@ -1255,14 +1242,9 @@
         (TOKEN_PARTS,),
         (2, TOKEN_PARTS),
         (4, TOKEN_PARTS),
-        (chunks, 3),
-        (chunks, 3),
-        (4, chunks),
-        (4, chunks),
-        (4, 2, 2),
-        (4, 3),
-        (4, 2),
     ]
+    shared = [(chunks, 3), (chunks, 3), (4, chunks), (4, chunks), (4, 2, 2), (4, 3), (4, 2)]
+    pairs = [(shape, shape) for shape in shapes] + [((1,), shape) for shape in shared]
     out = pl.pallas_call(
         pair_kernel,
         out_shape=jax.ShapeDtypeStruct((length, groups * local), BF16),
@@ -1299,7 +1281,7 @@
             pltpu.VMEM((4, length, local), BF16),
             pltpu.VMEM((4, length, local), BF16),
         ]
-        + [dma(shape) for shape in pairs for _ in range(2)]
+        + [dma(shape) for pair in pairs for shape in pair]
         + [dma((17,))],
         compiler_params=pltpu.CompilerParams(
             collective_id=0, has_side_effects=True, vmem_limit_bytes=VMEM_BYTES

time: 143 us -> 142 us (level)
  no operation moved by 1% of the time
where the time goes in v6:
time: 142 us; the launch traced here: 141 us
  Pallas kernels  137 us (96%)
  local copies, waits for them, and re-layouts  4.59 us (3%)
    pallas_call x1, Pallas kernels, pair_shards(): pl.pallas_call(pair_kernel, out_shape=jax.ShapeDtypeStruct((length, group...  137 us

profile of v6, /device:TPU:0, one launch (start us, length us, event | category | flops | bytes accessed | tf_op | source)
XLA Modules:
  0.0 141.4 jit_solution(8764052026340994485)
XLA Ops:
  0.0 2.1 %copy.16 = bf16[96,8,4,128]{3,1,2,0:T(8,128)(2,1)} copy(bf16[96,8,4,128]{3,2,1,0:T(4,128)(2,1)} %bitcast.6) | data formatting | bytes 1572864
  2.1 136.8 %shard_map.127 = bf16[768,512]{1,0:T(8,128)(2,1)} custom-call(bf16[768,512]{1,0:T(8,128)(2,1)} %bitcast.5, f32[4,128]{1,0:T(4,128)} %mixer_gain.1, f32[4,128]{1,0:T(4,128)} %pool_scale.1, f32[4,128]{1,0:T(4,128)} %channel_gain.1, f32[4,128]{1,0:T(4,128)} %down_scale_own.1, f32[1,384]{1,0:T(1,128)} %gate_scale.1, f32[1,384]{1,0:T(1,128)} %up_scale.1, ...), custom_call_target="tpu_custom_call" | custom-call | tf_op jit(solution)/shard_map/pallas_call | solution.py:1248
  139.0 2.4 %reshape.7 = bf16[1,768,4,128]{3,2,1,0:T(4,128)(2,1)} reshape(bf16[768,512]{1,0:T(8,128)(2,1)} %shard_map.127) | data formatting | bytes 1572864 | tf_op jit(solution)/shard_map/reshape | solution.py:1304
